TPU v7x, 32 devices: a whole 2x2x4 slice. The times are simulated.
32 devices in a mesh: grp: 2 (over x), ep: 16 (over z, y, core).
Axes of the slice: x: 2, y: 2, z: 4, core: 2. Of those that a mesh axis runs over, the one named last changes fastest.
Arguments:
- tokens: bfloat16 [1024, 2048], P(('grp', 'ep')), parts along dimension 0, may hold values from -6 to 6
- routes: int32 [1024, 4], P(('grp', 'ep')), parts along dimension 0, may hold values from 0 to 15, all different within a row; in each aligned block of 32 rows (0 to 31, 32 to 63, ...) at most 16 rows name the same one
- in_gain: float32 [2048], replicated, may hold values from 0.1 to 1.9
- group_router: float32 [2048, 4], replicated, may hold values from -0.03125 to 0.03125
- expert_router: float32 [2048, 16], replicated, may hold values from -0.03125 to 0.03125
- w_gate: bfloat16 [16, 2048, 512], P('ep'), may hold values from -0.125 to 0.125
- w_up: bfloat16 [16, 2048, 512], P('ep'), may hold values from -0.125 to 0.125
- w_down: bfloat16 [16, 512, 2048], P('ep')
- out_gain: float32 [2048], P('ep'), may hold values from 0.1 to 1.9
Outputs:
- mixed_out: bfloat16 [1024, 2048], P('grp', 'ep'), parts along dimension 0
There are 2 independent parts, one for each index of `grp`. A program takes and returns all parts, laid end to end along the dimension named above; an argument that names none is the same for every part. Nothing has to cross between parts.
Inputs may be any that keep to these rules, and one draw needn't show every extreme that they name: `routes`: each row names 4 different experts; in the rows of one device no expert is named more than 16 times, a bound that some block reaches.
All inputs are finite; a program needn't handle non-finite values.
Results may differ from a plain program's by a relative error of at most 0.0085.
Values may be sent and summed in bfloat16 or wider, within the bound.
No kernel may reach another device: no remote copies, remote signals or barrier semaphores. Data moves between devices by JAX's collectives and lax.ppermute only.
A program may use at most 64 MiB of HBM per device.

v0:
```python
import jax
import jax.numpy as jnp
from jax import lax
from jax.sharding import PartitionSpec as P

EPSILON = 1e-06


def normalize(tokens, in_gain):
    values = tokens.astype(jnp.float32)
    scaled = values * lax.rsqrt(jnp.mean(values * values, axis=1, keepdims=True) + EPSILON)
    return (scaled * in_gain).astype(jnp.bfloat16)


def gate_values(normed, routes, group_router, expert_router):
    wide = normed.astype(jnp.float32)
    group_logit = jnp.dot(wide, group_router, precision=lax.Precision.HIGHEST)
    expert_logit = jnp.dot(wide, expert_router, precision=lax.Precision.HIGHEST)
    group_prob = jnp.exp(group_logit) / jnp.sum(jnp.exp(group_logit), axis=1, keepdims=True)
    chosen = jnp.exp(jnp.take_along_axis(expert_logit, routes, axis=1))
    expert_prob = chosen / jnp.sum(chosen, axis=1, keepdims=True)
    per_group = expert_router.shape[1] // group_router.shape[1]
    return jnp.take_along_axis(group_prob, routes // per_group, axis=1) * expert_prob


def slot_order(pairs, experts):
    onehot = (pairs[:, :, None] == jnp.arange(experts, dtype=jnp.int32)).astype(jnp.int32)
    return jnp.sum(onehot * (jnp.cumsum(onehot, axis=1) - 1), axis=2)


def expert_rows(rows, w_gate, w_up, w_down):
    gate = jnp.dot(rows, w_gate[0], preferred_element_type=jnp.float32)
    upward = jnp.dot(rows, w_up[0], preferred_element_type=jnp.float32)
    hidden = (jax.nn.silu(gate) * upward).astype(jnp.bfloat16)
    return jnp.dot(hidden, w_down[0], preferred_element_type=jnp.float32).astype(jnp.bfloat16)


def per_device(
    tokens, routes, in_gain, group_router, expert_router, w_gate, w_up, w_down, out_gain
):
    tok_dev, top_count = routes.shape
    experts = expert_router.shape[1]
    capacity = 2 * tok_dev * top_count // experts
    normed = normalize(tokens, in_gain)
    weights = gate_values(normed, routes, group_router, expert_router)
    flat_route = routes.reshape(-1)
    order_in = slot_order(flat_route[None, :], experts)[0]
    slot_index = flat_route * capacity + order_in
    token_index = jnp.arange(tok_dev * top_count, dtype=jnp.int32) // top_count
    table = jnp.zeros((experts * capacity,), jnp.int32).at[slot_index].set(token_index)
    filled = jnp.zeros((experts * capacity,), jnp.bool_).at[slot_index].set(True)
    outgoing = jnp.where(filled[:, None], normed[table], jnp.zeros((), jnp.bfloat16))
    outgoing = outgoing.reshape(experts, capacity, normed.shape[1])
    arrived = lax.all_to_all(outgoing, "ep", split_axis=0, concat_axis=0, tiled=True)
    flat_rows = arrived.reshape(-1, arrived.shape[2])
    answer = expert_rows(flat_rows, w_gate, w_up, w_down).reshape(arrived.shape)
    returned = lax.all_to_all(answer, "ep", split_axis=0, concat_axis=0, tiled=True)
    pair_rows = returned.reshape(experts * capacity, normed.shape[1])[slot_index]
    weighted = pair_rows.astype(jnp.float32) * weights.reshape(-1)[:, None]
    mixed = jnp.sum(weighted.reshape(tok_dev, top_count, normed.shape[1]), axis=1)
    local_scale = lax.rsqrt(jnp.mean(mixed * mixed, axis=1, keepdims=True) + EPSILON)
    sending = mixed * local_scale
    part = lax.all_to_all(sending, "ep", split_axis=1, concat_axis=0, tiled=True)
    return (part * out_gain).astype(jnp.bfloat16)


def solution(mesh):
    in_specs = (
        P(("grp", "ep"), None),
        P(("grp", "ep"), None),
        P(),
        P(),
        P(),
        P("ep", None, None),
        P("ep", None, None),
        P("ep", None, None),
        P("ep"),
    )
    out_specs = P("grp", "ep")
    return jax.shard_map(
        per_device, mesh=mesh, in_specs=in_specs, out_specs=out_specs, check_vma=False
    )
```

profile of v0, /device:TPU:0, one launch (start us, length us, event | category | flops | bytes accessed | tf_op | source)
XLA Modules:
  0.0 95.3 jit_solution(5114007452190032896)
XLA Ops:
  0.0 0.0 copy-start
  0.0 0.8 broadcast_multiply_fusion
  0.8 0.8 copy.65
  1.6 1.0 %fusion.18 = f32[32]{0:T(128)S(1)} fusion(bf16[32,2048]{1,0:T(8,128)(2,1)} %param.9), kind=kLoop, calls=%fused_computation.24 | loop fusion | flops 196576 | bytes 131200 | tf_op jit(solution)/shard_map/reduce_sum | solution.py:11
  2.6 0.1 copy.64
  2.7 0.1 mul.83
  2.9 0.1 eq.27
  3.0 0.1 fusion.23
  3.1 0.2 reduce_window_sum.11
  3.2 0.2 select_reduce_fusion
  3.4 1.0 %scatter_custom_fusion.1 = s32[256]{0:T(256)S(1)} fusion(s32[128]{0:T(128)S(1)} %fusion.28, s32[128]{0:T(128)S(1)} %and_select_fusion, s32[]{:T(128)} %constant.70.clone.1), kind=kCustom, calls=%fused_computation.64 | custom fusion | bytes 1028 | tf_op jit(solution)/shard_map/scatter | solution.py:50
  4.4 1.0 %scatter_custom_fusion = pred[256]{0:T(512)(128)(4,1)S(1)} fusion(s32[128]{0:T(128)S(1)} %fusion.28, pred[128]{0:T(512)(128)(4,1)S(1)} %broadcast.205, pred[]{:T(512)} %constant.68.clone.1), kind=kCustom, calls=%fused_computation.59 | custom fusion | bytes 257 | tf_op jit(solution)/shard_map/scatter | solution.py:51
  5.4 0.1 broadcast_in_dim.42
  5.5 1.0 %fusion.20 = bf16[32,2048]{1,0:T(8,128)(2,1)S(1)} fusion(bf16[32,2048]{1,0:T(8,128)(2,1)} %param.9, f32[2048]{0:T(1024)} %param.11, f32[32]{0:T(128)S(1)} %add_rsqrt_fusion.1), kind=kLoop, calls=%fused_computation.26 | loop fusion | flops 262144 | bytes 270464 | tf_op jit(solution)/shard_map/convert_element_type | solution.py:12
  6.5 1.4 %gather_fusion = bf16[256,2048]{1,0:T(8,128)(2,1)S(1)} fusion(bf16[32,2048]{1,0:T(8,128)(2,1)S(1)} %fusion.20, s32[1024]{0:T(1024)S(1)} %pad_clamp_fusion.1), kind=kCustom, calls=%fused_computation | custom fusion | bytes 2098176 | tf_op jit(solution)/shard_map/gather | solution.py:52
  7.9 0.0 copy-start.5
  7.9 0.1 broadcast_select_fusion
  8.1 32.0 %all_to_all.26 = bf16[16,16,2048]{2,1,0:T(8,128)(2,1)S(1)} all-to-all(bf16[16,16,2048]{2,1,0:T(8,128)(2,1)S(1)} %broadcast_select_fusion), channel_id=1, replica_groups=mesh['grp'=2,'ep'=16] {'ep'}, dimensions={0} | all-to-all | bytes 2097152 | tf_op jit(solution)/shard_map/all_to_all | solution.py:54
  40.1 0.0 copy-done.5
  40.1 1.6 %fusion.3 = f32[256,512]{1,0:T(8,128)} fusion(bf16[256,2048]{1,0:T(8,128)(2,1)S(1)} %bitcast.54, bf16[1,2048,512]{2,1,0:T(8,128)(2,1)S(1)} %copy-done.5), kind=kOutput, calls=%fused_computation.10 | convolution fusion | flops 536870912 | bytes 3670016 | tf_op jit(solution)/shard_map/dot_general | solution.py:32
  41.7 0.0 copy-done
  41.7 4.0 %convolution_convert_fusion = bf16[256,2048]{1,0:T(8,128)(2,1)} fusion(bf16[1,512,2048]{2,1,0:T(8,128)(2,1)S(1)} %copy-done, bf16[256,2048]{1,0:T(8,128)(2,1)S(1)} %bitcast.55, bf16[1,2048,512]{2,1,0:T(8,128)(2,1)} %param.15, f32[256,512]{1,0:T(8,128)} %fusion.3), kind=kOutput, calls=%fused_computation.6 | convolution fusion | flops 1075052544 | bytes 6815744 | tf_op jit(solution)/shard_map/dot_general | solution.py:35
  45.7 0.0 copy-start.2
  45.7 0.0 copy-start.1
  45.7 5.2 %all-to-all-start.1 = ((bf16[16,16,2048]{2,1,0:T(8,128)(2,1)}), bf16[16,16,2048]{2,1,0:T(8,128)(2,1)S(1)}, u32[]{:S(2)}, u32[]{:S(2)}) async-start(bf16[16,16,2048]{2,1,0:T(8,128)(2,1)} %bitcast.53), calls=%async_computation.1 | async-start | bytes 2097152 | tf_op jit(solution)/shard_map/all_to_all | solution.py:57
  50.8 0.0 copy-done.2
  50.9 0.1 copy.68
  51.0 0.1 reshape.246
  51.1 0.1 copy.66
  51.2 0.1 reshape.240
  51.3 0.0 copy-done.1
  51.3 0.2 fusion.34
  51.5 0.0 copy-start.3
  51.5 1.4 %gather_fusion.3 = f32[128]{0:T(128)S(1)} fusion(f32[32,16]{0,1:T(8,128)S(1)} %fusion.34, s32[128]{0:T(128)S(1)} %reshape.246), kind=kCustom, calls=%fused_computation.3 | custom fusion | bytes 2048 | tf_op jit(solution)/shard_map/jit(take_along_axis)/gather | solution.py:20
  52.8 0.1 reshape.249
  52.9 0.1 copy.69
  53.0 0.0 copy-done.3
  53.0 0.2 fusion.33
  53.3 1.5 %gather_fusion.2 = f32[128]{0:T(128)S(1)} fusion(f32[32,4]{0,1:T(4,128)S(1)} %broadcast_divide_fusion, s32[128]{0:T(128)S(1)} %reshape.240), kind=kCustom, calls=%fused_computation.2 | custom fusion | bytes 2048 | tf_op jit(solution)/shard_map/jit(take_along_axis)/gather | solution.py:23
  54.8 0.1 reshape.243
  54.9 0.1 copy.67
  55.0 0.1 copy.70
  55.1 18.6 %all-to-all-done.1 = bf16[16,16,2048]{2,1,0:T(8,128)(2,1)S(1)} async-done(((bf16[16,16,2048]{2,1,0:T(8,128)(2,1)}), bf16[16,16,2048]{2,1,0:T(8,128)(2,1)S(1)}, u32[]{:S(2)}, u32[]{:S(2)}) %all-to-all-start.1) | async-done | bytes 1048608 | tf_op jit(solution)/shard_map/all_to_all | solution.py:57
  73.7 1.7 %gather_fusion.1 = bf16[128,2048]{1,0:T(8,128)(2,1)} fusion(bf16[256,2048]{1,0:T(8,128)(2,1)S(1)} %bitcast.50, s32[1024]{0:T(1024)S(1)} %pad_clamp_fusion), kind=kCustom, calls=%fused_computation.1 | custom fusion | bytes 1049088 | tf_op jit(solution)/shard_map/gather | solution.py:58
  75.5 1.4 %reshape.223 = f32[32,4,2048]{2,1,0:T(4,128)S(1)} reshape(bf16[128,2048]{1,0:T(8,128)(2,1)} %gather_fusion.1) | data formatting | bytes 1572864 | tf_op jit(solution)/shard_map/convert_element_type | solution.py:59
  76.8 0.0 copy-start.4
  76.8 0.7 multiply_reduce_fusion
  77.6 0.1 multiply_reduce_fusion.1
  77.7 0.1 copy.72
  77.8 0.1 bitcast_multiply_fusion
  77.9 0.1 copy.71
  78.0 16.6 %all_to_all.27 = f32[32,16,128]{2,0,1:T(8,128)S(1)} all-to-all(f32[32,16,128]{2,0,1:T(8,128)S(1)} %copy.71), channel_id=1, replica_groups=mesh['grp'=2,'ep'=16] {'ep'}, dimensions={1} | all-to-all | bytes 524288 | tf_op jit(solution)/shard_map/all_to_all | solution.py:63
  94.6 0.0 copy-done.4
  94.6 0.7 fusion.21
  (12 shorter events, 0.1 us)
Async XLA Ops:
  0.0 41.7 %copy-start = (bf16[1,512,2048]{2,1,0:T(8,128)(2,1)S(1)}, bf16[1,512,2048]{2,1,0:T(8,128)(2,1)}, u32[]{:S(2)}) copy-start(bf16[1,512,2048]{2,1,0:T(8,128)(2,1)} %param.16) | copy-start | bytes 6291460
  7.9 32.2 %copy-start.5 = (bf16[1,2048,512]{2,1,0:T(8,128)(2,1)S(1)}, bf16[1,2048,512]{2,1,0:T(8,128)(2,1)}, u32[]{:S(2)}) copy-start(bf16[1,2048,512]{2,1,0:T(8,128)(2,1)} %param.14) | copy-start | bytes 6291460
  45.7 5.2 %copy-start.2 = (s32[32,4]{0,1:T(4,128)S(1)}, s32[32,4]{0,1:T(4,128)}, u32[]{:S(2)}) copy-start(s32[32,4]{0,1:T(4,128)} %param.10) | copy-start | bytes 1540
  45.7 5.6 %copy-start.1 = (f32[2048,16]{0,1:T(8,128)S(1)}, f32[2048,16]{0,1:T(8,128)}, u32[]{:S(2)}) copy-start(f32[2048,16]{0,1:T(8,128)} %param.13) | copy-start | bytes 393220
  45.7 28.0 %all-to-all-start.1 = ((bf16[16,16,2048]{2,1,0:T(8,128)(2,1)}), bf16[16,16,2048]{2,1,0:T(8,128)(2,1)S(1)}, u32[]{:S(2)}, u32[]{:S(2)}) async-start(bf16[16,16,2048]{2,1,0:T(8,128)(2,1)} %bitcast.53), calls=%async_computation.1 | async-start | bytes 2097152 | tf_op jit(solution)/shard_map/all_to_all | solution.py:57
  51.5 1.5 %copy-start.3 = (f32[2048,4]{0,1:T(4,128)S(1)}, f32[2048,4]{0,1:T(4,128)}, u32[]{:S(2)}) copy-start(f32[2048,4]{0,1:T(4,128)} %param.12) | copy-start | bytes 98308
  76.8 17.8 %copy-start.4 = (f32[128]{0:T(128)S(1)}, f32[128]{0:T(128)}, u32[]{:S(2)}) copy-start(f32[128]{0:T(128)} %param.17) | copy-start | bytes 1540
where the time goes:
time: 95.7 us; the launch traced here: 95.3 us
  blocking collectives  48.6 us (51%)
  waiting for transfers between devices  18.6 us (19%)
  local copies, waits for them, and re-layouts  11.5 us (12%)
  matrix products  5.99 us (6%)
  other arithmetic  5.19 us (5%)
  starting transfers between devices  5.15 us (5%)
    all_to_all x1, blocking collectives, per_device(): lax.all_to_all(outgoing, 'ep', split_axis=0, concat_axis=0, tiled=True)  32 us
    all_to_all x1, waiting for transfers between devices, per_device(): lax.all_to_all(answer, 'ep', split_axis=0, concat_axis=0, tiled=True)  18.6 us
    all_to_all x1, blocking collectives, per_device(): lax.all_to_all(sending, 'ep', split_axis=1, concat_axis=0, tiled=True)  16.6 us
    all_to_all x1, starting transfers between devices, per_device(): lax.all_to_all(answer, 'ep', split_axis=0, concat_axis=0, tiled=True)  5.15 us
    dot_general x1, matrix products, expert_rows(): jnp.dot(hidden, w_down[0], preferred_element_type=jnp.float32)  4.01 us
  transfers between devices with their start and end apart: 1, of which 1 were waited for; matrix products, arithmetic and copies ran while one was open for 4% of the time, Pallas kernels for 0%

commit v1 on v0

v1 whole, which is shorter than its diff:
```python
import jax
import jax.numpy as jnp
from jax import lax
from jax.experimental import pallas as pl
from jax.experimental.pallas import tpu as pltpu
from jax.sharding import PartitionSpec as P

EPSILON = 1e-06
LANES = 128
F32 = jnp.float32
BF16 = jnp.bfloat16
NT = (((1,), (1,)), ((), ()))


def whole(count, memory=pltpu.VMEM):
    return [pl.BlockSpec(memory_space=memory)] * count


def payload_kernel(tokens, routes, in_gain, group_t, expert_t, out):
    values = tokens[...].astype(F32)
    width = values.shape[1]
    scaled = values * lax.rsqrt(jnp.mean(values * values, axis=1, keepdims=True) + EPSILON)
    normed = (scaled * in_gain[...]).astype(BF16)
    out[:, :width] = normed
    wide = normed.astype(F32)
    dot = lambda router: lax.dot_general(
        wide, router[...], NT, precision=lax.Precision.HIGHEST, preferred_element_type=F32
    )
    group_exp = jnp.exp(dot(group_t))
    expert_exp = jnp.exp(dot(expert_t))
    groups, experts = group_exp.shape[1], expert_exp.shape[1]
    group_prob = group_exp / jnp.sum(group_exp, axis=1, keepdims=True)
    lane = lax.broadcasted_iota(jnp.int32, expert_exp.shape, 1)
    chosen = jnp.zeros(expert_exp.shape, F32)
    for slot in range(routes.shape[1]):
        chosen = jnp.where(routes[:, slot : slot + 1] == lane, expert_exp, chosen)
    spread = jnp.zeros(expert_exp.shape, F32)
    for group in range(groups):
        spread = jnp.where(
            lane // (experts // groups) == group, group_prob[:, group : group + 1], spread
        )
    weight = spread * (chosen / jnp.sum(chosen, axis=1, keepdims=True))
    high = weight.astype(BF16)
    low = (weight - high.astype(F32)).astype(BF16)
    extra = out.shape[1] - width
    row = lax.broadcasted_iota(jnp.int32, (experts, extra), 0)
    column = lax.broadcasted_iota(jnp.int32, (experts, extra), 1)
    place = lambda shift: jnp.where(column == row + shift, 1.0, 0.0).astype(BF16)
    ext = jnp.dot(high, place(0), preferred_element_type=F32)
    ext = ext + jnp.dot(low, place(experts), preferred_element_type=F32)
    out[:, width:] = ext.astype(BF16)


def expert_body(far, width, experts, block):
    def kernel(where_at, *refs):
        near_refs, peer_refs = refs[:far], refs[far : 2 * far]
        w_gate, w_up, w_down = refs[2 * far : 2 * far + 3]
        keep, send = refs[2 * far + 3 : 3 * far + 3], refs[3 * far + 3 : 4 * far + 3]
        rows, result = refs[4 * far + 3], refs[4 * far + 4]
        mine = where_at[0]
        top, mid, low = mine // 4, (mine // 2) % 2, mine % 2
        tok = near_refs[0].shape[1]
        for q in range(far):
            for s in range(2):
                base = ((top + far - q) % far) * 4 + (mid ^ s) * 2
                for r, ref in ((0, near_refs[q]), (1, peer_refs[q])):
                    at = pl.multiple_of((base + (low ^ r)) * tok, tok)
                    rows[pl.ds(at, tok), :] = ref[s]
        ext = rows[:, width:].astype(F32)
        lane = lax.broadcasted_iota(jnp.int32, ext.shape, 1)
        hit = (lane == mine) | (lane == mine + experts)
        weight = jnp.sum(jnp.where(hit, ext, 0.0), axis=1, keepdims=True)
        data = rows[:, :width]
        gate = jnp.dot(data, w_gate[0], preferred_element_type=F32)
        upward = jnp.dot(data, w_up[0], preferred_element_type=F32)
        hidden = (gate / (1.0 + jnp.exp(-gate)) * upward * weight).astype(BF16)
        result[...] = jnp.dot(hidden, w_down[0], preferred_element_type=F32).astype(BF16)
        for q in range(far):
            for s in range(2):
                at = (((top + q) % far) * 2 + (mid ^ s)) * 2 * block
                pair = result[:, pl.ds(pl.multiple_of(at, 2 * block), 2 * block)]
                left, right = pair[:, :block], pair[:, block:]
                keep[q][s] = jnp.where(low == 0, left, right)
                send[q][s] = jnp.where(low == 0, right, left)

    return kernel


def add(one, two):
    return (one.astype(F32) + two.astype(F32)).astype(BF16)


def per_device(
    tokens, routes, in_gain, group_router, expert_router, w_gate, w_up, w_down, out_gain
):
    tok, width = tokens.shape
    experts = expert_router.shape[1]
    ep = lax.axis_size("ep")
    far, block = ep // 4, width // ep
    extra = -(-2 * experts // LANES) * LANES
    mine = lax.axis_index("ep").astype(jnp.int32)

    def flip(value, bit):
        return lax.ppermute(value, "ep", [(i, i ^ bit) for i in range(ep)])

    def shift(value, step):
        moves = [(i, ((i // 4 + step) % far) * 4 + i % 4) for i in range(ep)]
        return lax.ppermute(value, "ep", moves)

    payload = pl.pallas_call(
        payload_kernel,
        out_shape=jax.ShapeDtypeStruct((tok, width + extra), BF16),
        in_specs=whole(5),
        out_specs=pl.BlockSpec(memory_space=pltpu.VMEM),
    )(tokens, routes, in_gain[None, :], group_router.T, expert_router.T)

    steps = [1, far - 1] + [q for q in range(2, far - 1)]
    held = {0: payload}
    for q in steps:
        held[q] = shift(payload, q)
    near, peer = {}, {}
    for q in [0] + steps:
        near[q] = jnp.stack([held[q], flip(held[q], 2)])
        peer[q] = flip(near[q], 1)
    total = ep * tok
    piece = jax.ShapeDtypeStruct((2, total, block), BF16)
    parts = pl.pallas_call(
        expert_body(far, width, experts, block),
        out_shape=[piece] * (2 * far),
        in_specs=whole(1, pltpu.SMEM) + whole(2 * far + 3),
        out_specs=whole(2 * far),
        scratch_shapes=[
            pltpu.VMEM((total, width + extra), BF16),
            pltpu.VMEM((total, width), BF16),
        ],
    )(
        mine[None],
        *[near[q] for q in range(far)],
        *[peer[q] for q in range(far)],
        w_gate,
        w_up,
        w_down,
    )
    keep, send = parts[:far], parts[far:]
    order = [q for q in range(2, far - 1)] + [1, far - 1, 0]
    landed = {}
    for q in order:
        paired = add(keep[q], flip(send[q], 1))
        squared = add(paired[0], flip(paired[1], 2))
        landed[q] = shift(squared, q) if q else squared
    mixed = landed[0].astype(F32)
    for q in order[:-1]:
        mixed = mixed + landed[q].astype(F32)
    power = jnp.sum(mixed * mixed, axis=1)
    power = power + flip(power, 1)
    power = power + flip(power, 2)
    others = [shift(power, q) for q in range(1, far)]
    for other in others:
        power = power + other
    scale = lax.rsqrt(power / width + EPSILON)
    return (mixed * scale[:, None] * out_gain).astype(BF16)


def solution(mesh):
    in_specs = (
        P(("grp", "ep"), None),
        P(("grp", "ep"), None),
        P(),
        P(),
        P(),
        P("ep", None, None),
        P("ep", None, None),
        P("ep", None, None),
        P("ep"),
    )
    out_specs = P("grp", "ep")
    return jax.shard_map(
        per_device, mesh=mesh, in_specs=in_specs, out_specs=out_specs, check_vma=False
    )
```

time: 95.7 us -> 79.8 us (0.83)
  blocking collectives: 48.6 us -> 0 us
  starting transfers between devices: 5.15 us -> 30.5 us
  waiting for transfers between devices: 18.6 us -> 31 us
  Pallas kernels: 0 us -> 11.4 us
  local copies, waits for them, and re-layouts: 11.5 us -> 2.11 us
  matrix products: 5.99 us -> 0 us
    all_to_all x2 -> x0, blocking collectives: 48.6 us -> none  [the longest x1 32 us: per_device(): lax.all_to_all(outgoing, 'ep', split_axis=0, concat_axis=0, tiled=True)]
    ppermute x0 -> x27, waiting for transfers between devices: none -> 31 us  [the longest x9 17.8 us: shift(): return lax.ppermute(value, 'ep', moves)]
    ppermute x0 -> x27, starting transfers between devices: none -> 30.5 us  [the longest x9 17.5 us: shift(): return lax.ppermute(value, 'ep', moves)]
    all_to_all x1 -> x0, waiting for transfers between devices: 18.6 us -> none  [per_device(): lax.all_to_all(answer, 'ep', split_axis=0, concat_axis=0, tiled=True)]
    pallas_call x0 -> x2, Pallas kernels: none -> 11.4 us  [the longest x1 8.7 us: per_device(): pl.pallas_call(expert_body(far, width, experts, block), out_shape=[piece]...]
    gather x12 -> x0, local copies, waits for them, and re-layouts: 6.68 us -> none  [the longest x5 1.88 us: gate_values(): jnp.take_along_axis(group_prob, routes // per_group, axis=1) * expert_prob]
    dot_general x4 -> x0, matrix products: 5.99 us -> none  [the longest x1 4.01 us: expert_rows(): jnp.dot(hidden, w_down[0], preferred_element_type=jnp.float32)]
    all_to_all x1 -> x0, starting transfers between devices: 5.15 us -> none  [per_device(): lax.all_to_all(answer, 'ep', split_axis=0, concat_axis=0, tiled=True)]
  transfers between devices with their start and end apart: 1 -> 27, of which waited for: 1 -> 14; matrix products, arithmetic and copies ran while one was open for 4% -> 4% of each run, Pallas kernels for 0% -> 0%
where the time goes in v1:
time: 79.8 us; the launch traced here: 79.5 us
  waiting for transfers between devices  31 us (39%)
  starting transfers between devices  30.5 us (38%)
  Pallas kernels  11.4 us (14%)
  other arithmetic  4.32 us (5%)
  local copies, waits for them, and re-layouts  2.11 us (3%)
    ppermute x9, waiting for transfers between devices, shift(): return lax.ppermute(value, 'ep', moves)  17.8 us
    ppermute x9, starting transfers between devices, shift(): return lax.ppermute(value, 'ep', moves)  17.5 us
    ppermute x18, waiting for transfers between devices, flip(): return lax.ppermute(value, 'ep', [(i, i ^ bit) for i in range(ep)])  13.2 us
    ppermute x18, starting transfers between devices, flip(): return lax.ppermute(value, 'ep', [(i, i ^ bit) for i in range(ep)])  13 us
    pallas_call x1, Pallas kernels, per_device(): pl.pallas_call(expert_body(far, width, experts, block), out_shape=[piece]...  8.7 us
    pallas_call x1, Pallas kernels, per_device(): pl.pallas_call(payload_kernel, out_shape=jax.ShapeDtypeStruct((tok, width...  2.68 us
    convert_element_type x7, other arithmetic, add(): return (one.astype(F32) + two.astype(F32)).astype(BF16)  2.3 us
    unnamed x23, local copies, waits for them, and re-layouts  2.07 us
  transfers between devices with their start and end apart: 27, of which 14 were waited for; matrix products, arithmetic and copies ran while one was open for 4% of the time, Pallas kernels for 0%

profile of v1, /device:TPU:0, one launch (start us, length us, event | category | flops | bytes accessed | tf_op | source)
XLA Modules:
  0.0 79.5 jit_solution(1346521853854696913)
XLA Ops:
  0.0 1.4 %copy.10.routes = s32[32,4]{1,0:T(8,128)} copy(s32[32,4]{0,1:T(4,128)} %param.10) | data formatting | bytes 1024 | tf_op args[1]
  1.4 2.7 %shard_map.91 = bf16[32,2176]{1,0:T(8,128)(2,1)} custom-call(bf16[32,2048]{1,0:T(8,128)(2,1)} %tokens.1, s32[32,4]{1,0:T(8,128)} %copy.10.routes, f32[1,2048]{1,0:T(1,128)} %bitcast.54, f32[4,2048]{1,0:T(4,128)} %bitcast.53, f32[16,2048]{1,0:T(8,128)} %bitcast.52), custom_call_target="tpu_custom_call" | custom-call | tf_op jit(solution)/shard_map/pallas_call | solution.py:110
  4.0 3.0 %collective-permute-start.1 = (bf16[32,2176]{1,0:T(8,128)(2,1)}, bf16[32,2176]{1,0:T(8,128)(2,1)S(1)}, u32[]{:S(2)}, u32[]{:S(2)}) collective-permute-start(bf16[32,2176]{1,0:T(8,128)(2,1)} %shard_map.91), channel_id=1, source_target_pairs={{0,4},{1,5},{2,6},{3,7},{4,8},{5,9},{6,10},{7,11},{8,12},{9,13},{1... | collective-permute-start | bytes 417800 | tf_op jit(solution)/shard_map/ppermute | solution.py:108
  7.1 1.5 %collective-permute-start = (bf16[32,2176]{1,0:T(8,128)(2,1)}, bf16[32,2176]{1,0:T(8,128)(2,1)S(1)}, u32[]{:S(2)}, u32[]{:S(2)}) collective-permute-start(bf16[32,2176]{1,0:T(8,128)(2,1)} %shard_map.91), channel_id=1, source_target_pairs={{0,2},{1,3},{2,0},{3,1},{4,6},{5,7},{6,4},{7,5},{8,10},{9,11},{10,... | collective-permute-start | bytes 417800 | tf_op jit(solution)/shard_map/ppermute | solution.py:104
  8.6 2.2 %collective-permute-start.5 = (bf16[32,2176]{1,0:T(8,128)(2,1)}, bf16[32,2176]{1,0:T(8,128)(2,1)S(1)}, u32[]{:S(2)}, u32[]{:S(2)}) collective-permute-start(bf16[32,2176]{1,0:T(8,128)(2,1)} %shard_map.91), channel_id=1, source_target_pairs={{0,12},{1,13},{2,14},{3,15},{4,0},{5,1},{6,2},{7,3},{8,4},{9,5},{1... | collective-permute-start | bytes 417800 | tf_op jit(solution)/shard_map/ppermute | solution.py:108
  10.9 0.8 collective-permute-start.3
  11.7 1.6 %collective-permute-done.1 = bf16[32,2176]{1,0:T(8,128)(2,1)S(1)} collective-permute-done((bf16[32,2176]{1,0:T(8,128)(2,1)}, bf16[32,2176]{1,0:T(8,128)(2,1)S(1)}, u32[]{:S(2)}, u32[]{:S(2)}) %collective-permute-start.1) | collective-permute-done | bytes 139296 | tf_op jit(solution)/shard_map/ppermute | solution.py:108
  13.3 2.3 %collective-permute-start.2 = (bf16[32,2176]{1,0:T(8,128)(2,1)S(1)}, bf16[32,2176]{1,0:T(8,128)(2,1)S(1)}, u32[]{:S(2)}, u32[]{:S(2)}) collective-permute-start(bf16[32,2176]{1,0:T(8,128)(2,1)S(1)} %collective-permute-done.1), channel_id=1, source_target_pairs={{0,2},{1,3},{2,0},{3,1},{4,6},{5,7},{6,4},{7,5},{8,10},{9,11},{10,... | collective-permute-start | bytes 417800 | tf_op jit(solution)/shard_map/ppermute | solution.py:104
  15.6 0.0 collective-permute-done
  15.6 0.9 %pad_maximum_fusion.refs_0_ = bf16[2,32,2176]{2,1,0:T(8,128)(2,1)S(1)} fusion(bf16[1,32,2176]{2,1,0:T(8,128)(2,1)S(1)} %bitcast.50, bf16[1,32,2176]{2,1,0:T(8,128)(2,1)} %bitcast.44), kind=kLoop, calls=%fused_computation.4 | loop fusion | flops 139264 | bytes 557056 | tf_op jit(solution)/shard_map/stack | solution.py:123
  16.6 0.1 collective-permute-start.7
  16.6 0.0 collective-permute-done.5
  16.6 0.5 collective-permute-start.6
  17.2 4.8 %collective-permute-done.3 = bf16[32,2176]{1,0:T(8,128)(2,1)S(1)} collective-permute-done((bf16[32,2176]{1,0:T(8,128)(2,1)}, bf16[32,2176]{1,0:T(8,128)(2,1)S(1)}, u32[]{:S(2)}, u32[]{:S(2)}) %collective-permute-start.3) | collective-permute-done | bytes 139296 | tf_op jit(solution)/shard_map/ppermute | solution.py:108
  22.0 1.5 %collective-permute-start.4 = (bf16[32,2176]{1,0:T(8,128)(2,1)S(1)}, bf16[32,2176]{1,0:T(8,128)(2,1)S(1)}, u32[]{:S(2)}, u32[]{:S(2)}) collective-permute-start(bf16[32,2176]{1,0:T(8,128)(2,1)S(1)} %collective-permute-done.3), channel_id=1, source_target_pairs={{0,2},{1,3},{2,0},{3,1},{4,6},{5,7},{6,4},{7,5},{8,10},{9,11},{10,... | collective-permute-start | bytes 417800 | tf_op jit(solution)/shard_map/ppermute | solution.py:104
  23.5 0.0 collective-permute-done.2
  23.5 0.1 collective-permute-start.8
  23.6 3.6 %collective-permute-done.4 = bf16[32,2176]{1,0:T(8,128)(2,1)S(1)} collective-permute-done((bf16[32,2176]{1,0:T(8,128)(2,1)S(1)}, bf16[32,2176]{1,0:T(8,128)(2,1)S(1)}, u32[]{:S(2)}, u32[]{:S(2)}) %collective-permute-start.4) | collective-permute-done | bytes 139296 | tf_op jit(solution)/shard_map/ppermute | solution.py:104
  27.3 0.1 collective-permute-start.9
  27.4 0.0 collective-permute-done.6
  27.4 0.6 collective-permute-start.10
  28.0 0.0 collective-permute-done.7.refs_4_
  28.0 0.0 collective-permute-done.8.refs_5_
  28.0 0.9 %collective-permute-done.9.refs_6_ = bf16[2,32,2176]{2,1,0:T(8,128)(2,1)S(1)} collective-permute-done((bf16[2,32,2176]{2,1,0:T(8,128)(2,1)S(1)}, bf16[2,32,2176]{2,1,0:T(8,128)(2,1)S(1)}, u32[]{:S(2)}, u32[]{:S(2)}) %collective-permute-start.9) | collective-permute-done | bytes 278560 | tf_op jit(solution)/shard_map/ppermute | solution.py:104
  28.9 0.4 collective-permute-done.10.refs_7_
  29.4 0.3 copy-done.6
  29.6 0.4 copy-done.7
  30.0 8.7 %shard_map.92 = (bf16[2,512,128]{2,1,0:T(8,128)(2,1)}, bf16[2,512,128]{2,1,0:T(8,128)(2,1)}, bf16[2,512,128]{2,1,0:T(8,128)(2,1)}, bf16[2,512,128]{2,1,0:T(8,128...) custom-call(s32[1]{0:T(128)} %bitcast.where_at, ...), custom_call_target="tpu_custom_call" | custom-call | tf_op jit(solution)/shard_map/pallas_call | solution.py:127
  38.7 0.3 collective-permute-start.11
  39.0 0.3 collective-permute-start.13
  39.3 0.2 collective-permute-start.16
  39.5 0.3 collective-permute-start.19
  39.8 0.7 collective-permute-done.11
  40.5 1.0 %add_convert_fusion.3 = bf16[2,512,128]{2,1,0:T(8,128)(2,1)S(1)} fusion(bf16[2,512,128]{2,1,0:T(8,128)(2,1)S(1)} %collective-permute-done.11, bf16[2,512,128]{2,1,0:T(8,128)(2,1)} %get-tuple-element.13), kind=kLoop, calls=%fused_computation.3 | loop fusion | flops 524288 | bytes 786432 | tf_op jit(solution)/shard_map/convert_element_type | solution.py:90
  41.6 1.7 %collective-permute-start.12 = (bf16[512,128]{1,0:T(8,128)(2,1)S(1)}, bf16[512,128]{1,0:T(8,128)(2,1)S(1)}, u32[]{:S(2)}, u32[]{:S(2)}) collective-permute-start(bf16[512,128]{1,0:T(8,128)(2,1)S(1)} %slice_bitcast_fusion.6), channel_id=1, source_target_pairs={{0,2},{1,3},{2,0},{3,1},{4,6},{5,7},{6,4},{7,5},{8,10},{9,11},{10,... | collective-permute-start | bytes 393224 | tf_op jit(solution)/shard_map/ppermute | solution.py:104
  43.3 0.0 collective-permute-done.13
  43.3 1.0 %add_convert_fusion.2 = bf16[2,512,128]{2,1,0:T(8,128)(2,1)S(1)} fusion(bf16[2,512,128]{2,1,0:T(8,128)(2,1)S(1)} %collective-permute-done.13, bf16[2,512,128]{2,1,0:T(8,128)(2,1)} %get-tuple-element.15), kind=kLoop, calls=%fused_computation.2 | loop fusion | flops 524288 | bytes 786432 | tf_op jit(solution)/shard_map/convert_element_type | solution.py:90
  44.4 0.0 copy-start.10
  44.4 0.4 collective-permute-start.14
  44.8 0.0 collective-permute-done.16
  44.8 0.1 add_convert_fusion.1
  44.9 1.7 %collective-permute-start.17 = (bf16[512,128]{1,0:T(8,128)(2,1)S(1)}, bf16[512,128]{1,0:T(8,128)(2,1)S(1)}, u32[]{:S(2)}, u32[]{:S(2)}) collective-permute-start(bf16[512,128]{1,0:T(8,128)(2,1)S(1)} %slice_bitcast_fusion.2), channel_id=1, source_target_pairs={{0,2},{1,3},{2,0},{3,1},{4,6},{5,7},{6,4},{7,5},{8,10},{9,11},{10,... | collective-permute-start | bytes 393224 | tf_op jit(solution)/shard_map/ppermute | solution.py:104
  46.6 0.0 collective-permute-done.19
  46.6 0.1 add_convert_fusion
  46.7 0.4 collective-permute-start.20
  47.2 3.7 %collective-permute-done.14 = bf16[512,128]{1,0:T(8,128)(2,1)S(1)} collective-permute-done((bf16[512,128]{1,0:T(8,128)(2,1)S(1)}, bf16[512,128]{1,0:T(8,128)(2,1)S(1)}, u32[]{:S(2)}, u32[]{:S(2)}) %collective-permute-start.14) | collective-permute-done | bytes 131104 | tf_op jit(solution)/shard_map/ppermute | solution.py:104
  50.9 4.7 %collective-permute-start.15 = (bf16[512,128]{1,0:T(8,128)(2,1)S(1)}, bf16[512,128]{1,0:T(8,128)(2,1)S(1)}, u32[]{:S(2)}, u32[]{:S(2)}) collective-permute-start(bf16[512,128]{1,0:T(8,128)(2,1)S(1)} %fusion.2), channel_id=1, source_target_pairs={{0,8},{1,9},{2,10},{3,11},{4,12},{5,13},{6,14},{7,15},{8,0},{9,1},... | collective-permute-start | bytes 393224 | tf_op jit(solution)/shard_map/ppermute | solution.py:108
  55.6 0.8 collective-permute-start.18
  56.4 3.1 %collective-permute-start.21 = (bf16[512,128]{1,0:T(8,128)(2,1)S(1)}, bf16[512,128]{1,0:T(8,128)(2,1)S(1)}, u32[]{:S(2)}, u32[]{:S(2)}) collective-permute-start(bf16[512,128]{1,0:T(8,128)(2,1)S(1)} %fusion), channel_id=1, source_target_pairs={{0,12},{1,13},{2,14},{3,15},{4,0},{5,1},{6,2},{7,3},{8,4},{9,5},{1... | collective-permute-start | bytes 393224 | tf_op jit(solution)/shard_map/ppermute | solution.py:108
  59.6 4.6 %collective-permute-done.15 = bf16[512,128]{1,0:T(8,128)(2,1)S(1)} collective-permute-done((bf16[512,128]{1,0:T(8,128)(2,1)S(1)}, bf16[512,128]{1,0:T(8,128)(2,1)S(1)}, u32[]{:S(2)}, u32[]{:S(2)}) %collective-permute-start.15) | collective-permute-done | bytes 131104 | tf_op jit(solution)/shard_map/ppermute | solution.py:108
  64.2 0.0 collective-permute-done.18
  64.2 1.7 %collective-permute-done.21 = bf16[512,128]{1,0:T(8,128)(2,1)S(1)} collective-permute-done((bf16[512,128]{1,0:T(8,128)(2,1)S(1)}, bf16[512,128]{1,0:T(8,128)(2,1)S(1)}, u32[]{:S(2)}, u32[]{:S(2)}) %collective-permute-start.21) | collective-permute-done | bytes 131104 | tf_op jit(solution)/shard_map/ppermute | solution.py:108
  65.9 0.2 multiply_reduce_fusion
  66.0 0.1 collective-permute-start.22
  66.1 1.1 %collective-permute-done.22 = f32[512]{0:T(512)S(1)} collective-permute-done((f32[512]{0:T(512)S(1)}, f32[512]{0:T(512)S(1)}, u32[]{:S(2)}, u32[]{:S(2)}) %collective-permute-start.22) | collective-permute-done | bytes 2080 | tf_op jit(solution)/shard_map/ppermute | solution.py:104
  67.3 0.9 %collective-permute-start.23 = (f32[512]{0:T(512)S(1)}, f32[512]{0:T(512)S(1)}, u32[]{:S(2)}, u32[]{:S(2)}) collective-permute-start(f32[512]{0:T(512)S(1)} %add.65), channel_id=1, source_target_pairs={{0,2},{1,3},{2,0},{3,1},{4,6},{5,7},{6,4},{7,5},{8,10},{9,11},{10,... | collective-permute-start | bytes 6152 | tf_op jit(solution)/shard_map/ppermute | solution.py:104
  68.2 2.7 %collective-permute-done.23 = f32[512]{0:T(512)S(1)} collective-permute-done((f32[512]{0:T(512)S(1)}, f32[512]{0:T(512)S(1)}, u32[]{:S(2)}, u32[]{:S(2)}) %collective-permute-start.23) | collective-permute-done | bytes 2080 | tf_op jit(solution)/shard_map/ppermute | solution.py:104
  70.9 1.3 %collective-permute-start.26 = (f32[512]{0:T(512)S(1)}, f32[512]{0:T(512)S(1)}, u32[]{:S(2)}, u32[]{:S(2)}) collective-permute-start(f32[512]{0:T(512)S(1)} %add.66), channel_id=1, source_target_pairs={{0,12},{1,13},{2,14},{3,15},{4,0},{5,1},{6,2},{7,3},{8,4},{9,5},{1... | collective-permute-start | bytes 6152 | tf_op jit(solution)/shard_map/ppermute | solution.py:108
  72.2 1.2 %collective-permute-start.25 = (f32[512]{0:T(512)S(1)}, f32[512]{0:T(512)S(1)}, u32[]{:S(2)}, u32[]{:S(2)}) collective-permute-start(f32[512]{0:T(512)S(1)} %add.66), channel_id=1, source_target_pairs={{0,8},{1,9},{2,10},{3,11},{4,12},{5,13},{6,14},{7,15},{8,0},{9,1},... | collective-permute-start | bytes 6152 | tf_op jit(solution)/shard_map/ppermute | solution.py:108
  73.3 0.3 collective-permute-start.24
  73.6 0.8 %collective-permute-done.26 = f32[512]{0:T(512)S(1)} collective-permute-done((f32[512]{0:T(512)S(1)}, f32[512]{0:T(512)S(1)}, u32[]{:S(2)}, u32[]{:S(2)}) %collective-permute-start.26) | collective-permute-done | bytes 2080 | tf_op jit(solution)/shard_map/ppermute | solution.py:108
  74.5 2.2 %collective-permute-done.25 = f32[512]{0:T(512)S(1)} collective-permute-done((f32[512]{0:T(512)S(1)}, f32[512]{0:T(512)S(1)}, u32[]{:S(2)}, u32[]{:S(2)}) %collective-permute-start.25) | collective-permute-done | bytes 2080 | tf_op jit(solution)/shard_map/ppermute | solution.py:108
  76.7 2.1 %collective-permute-done.24 = f32[512]{0:T(512)S(1)} collective-permute-done((f32[512]{0:T(512)S(1)}, f32[512]{0:T(512)S(1)}, u32[]{:S(2)}, u32[]{:S(2)}) %collective-permute-start.24) | collective-permute-done | bytes 2080 | tf_op jit(solution)/shard_map/ppermute | solution.py:108
  78.7 0.8 %multiply_convert_fusion = bf16[512,128]{1,0:T(8,128)(2,1)} fusion(f32[128]{0:T(128)S(1)} %copy-done.10, f32[512]{0:T(512)S(1)} %add_rsqrt_fusion, bf16[512,128]{1,0:T(8,128)(2,1)S(1)} %collective-permute-done.21, bf16[512,128]{1,0:T(8,128)(2,1)S(1)} %collective-permute-done.18, bf16[512,128]{1,0:T(8,128)(2,1)S(1)} %collective-permute-done.15, ...), kind=kLoop, calls=%fused_computation.16 | loop fusion | flops 917504 | bytes 788992 | tf_op jit(solution)/shard_map/convert_element_type | solution.py:161
  (35 shorter events, 0.3 us)
Async XLA Ops:
  4.0 9.2 %collective-permute-start.1 = (bf16[32,2176]{1,0:T(8,128)(2,1)}, bf16[32,2176]{1,0:T(8,128)(2,1)S(1)}, u32[]{:S(2)}, u32[]{:S(2)}) collective-permute-start(bf16[32,2176]{1,0:T(8,128)(2,1)} %shard_map.91), channel_id=1, source_target_pairs={{0,4},{1,5},{2,6},{3,7},{4,8},{5,9},{6,10},{7,11},{8,12},{9,13},{1... | collective-permute-start | bytes 417800 | tf_op jit(solution)/shard_map/ppermute | solution.py:108
  7.1 8.5 %collective-permute-start = (bf16[32,2176]{1,0:T(8,128)(2,1)}, bf16[32,2176]{1,0:T(8,128)(2,1)S(1)}, u32[]{:S(2)}, u32[]{:S(2)}) collective-permute-start(bf16[32,2176]{1,0:T(8,128)(2,1)} %shard_map.91), channel_id=1, source_target_pairs={{0,2},{1,3},{2,0},{3,1},{4,6},{5,7},{6,4},{7,5},{8,10},{9,11},{10,... | collective-permute-start | bytes 417800 | tf_op jit(solution)/shard_map/ppermute | solution.py:104
  8.6 8.0 %collective-permute-start.5 = (bf16[32,2176]{1,0:T(8,128)(2,1)}, bf16[32,2176]{1,0:T(8,128)(2,1)S(1)}, u32[]{:S(2)}, u32[]{:S(2)}) collective-permute-start(bf16[32,2176]{1,0:T(8,128)(2,1)} %shard_map.91), channel_id=1, source_target_pairs={{0,12},{1,13},{2,14},{3,15},{4,0},{5,1},{6,2},{7,3},{8,4},{9,5},{1... | collective-permute-start | bytes 417800 | tf_op jit(solution)/shard_map/ppermute | solution.py:108
  10.9 11.1 %collective-permute-start.3 = (bf16[32,2176]{1,0:T(8,128)(2,1)}, bf16[32,2176]{1,0:T(8,128)(2,1)S(1)}, u32[]{:S(2)}, u32[]{:S(2)}) collective-permute-start(bf16[32,2176]{1,0:T(8,128)(2,1)} %shard_map.91), channel_id=1, source_target_pairs={{0,8},{1,9},{2,10},{3,11},{4,12},{5,13},{6,14},{7,15},{8,0},{9,1},... | collective-permute-start | bytes 417800 | tf_op jit(solution)/shard_map/ppermute | solution.py:108
  13.3 10.2 %collective-permute-start.2 = (bf16[32,2176]{1,0:T(8,128)(2,1)S(1)}, bf16[32,2176]{1,0:T(8,128)(2,1)S(1)}, u32[]{:S(2)}, u32[]{:S(2)}) collective-permute-start(bf16[32,2176]{1,0:T(8,128)(2,1)S(1)} %collective-permute-done.1), channel_id=1, source_target_pairs={{0,2},{1,3},{2,0},{3,1},{4,6},{5,7},{6,4},{7,5},{8,10},{9,11},{10,... | collective-permute-start | bytes 417800 | tf_op jit(solution)/shard_map/ppermute | solution.py:104
  16.5 12.8 %copy-start = (bf16[2,32,2176]{2,1,0:T(8,128)(2,1)}, bf16[2,32,2176]{2,1,0:T(8,128)(2,1)S(1)}, u32[]{:S(2)}) copy-start(bf16[2,32,2176]{2,1,0:T(8,128)(2,1)S(1)} %pad_maximum_fusion.refs_0_) | copy-start | bytes 835588
  16.6 11.4 %collective-permute-start.7 = (bf16[2,32,2176]{2,1,0:T(8,128)(2,1)S(1)}, bf16[2,32,2176]{2,1,0:T(8,128)(2,1)S(1)}, u32[]{:S(2)}, u32[]{:S(2)}) collective-permute-start(bf16[2,32,2176]{2,1,0:T(8,128)(2,1)S(1)} %pad_maximum_fusion.refs_0_), channel_id=1, source_target_pairs={{0,1},{1,0},{2,3},{3,2},{4,5},{5,4},{6,7},{7,6},{8,9},{9,8},{10,11... | collective-permute-start | bytes 835592 | tf_op jit(solution)/shard_map/ppermute | solution.py:104
  16.6 10.7 %collective-permute-start.6 = (bf16[32,2176]{1,0:T(8,128)(2,1)S(1)}, bf16[32,2176]{1,0:T(8,128)(2,1)S(1)}, u32[]{:S(2)}, u32[]{:S(2)}) collective-permute-start(bf16[32,2176]{1,0:T(8,128)(2,1)S(1)} %collective-permute-done.5), channel_id=1, source_target_pairs={{0,2},{1,3},{2,0},{3,1},{4,6},{5,7},{6,4},{7,5},{8,10},{9,11},{10,... | collective-permute-start | bytes 417800 | tf_op jit(solution)/shard_map/ppermute | solution.py:104
  22.0 5.3 %collective-permute-start.4 = (bf16[32,2176]{1,0:T(8,128)(2,1)S(1)}, bf16[32,2176]{1,0:T(8,128)(2,1)S(1)}, u32[]{:S(2)}, u32[]{:S(2)}) collective-permute-start(bf16[32,2176]{1,0:T(8,128)(2,1)S(1)} %collective-permute-done.3), channel_id=1, source_target_pairs={{0,2},{1,3},{2,0},{3,1},{4,6},{5,7},{6,4},{7,5},{8,10},{9,11},{10,... | collective-permute-start | bytes 417800 | tf_op jit(solution)/shard_map/ppermute | solution.py:104
  23.5 5.8 %copy-start.1 = (bf16[2,32,2176]{2,1,0:T(8,128)(2,1)}, bf16[2,32,2176]{2,1,0:T(8,128)(2,1)S(1)}, u32[]{:S(2)}) copy-start(bf16[2,32,2176]{2,1,0:T(8,128)(2,1)S(1)} %pad_maximum_fusion.1.refs_1_) | copy-start | bytes 835588
  23.5 4.5 %collective-permute-start.8 = (bf16[2,32,2176]{2,1,0:T(8,128)(2,1)S(1)}, bf16[2,32,2176]{2,1,0:T(8,128)(2,1)S(1)}, u32[]{:S(2)}, u32[]{:S(2)}) collective-permute-start(bf16[2,32,2176]{2,1,0:T(8,128)(2,1)S(1)} %pad_maximum_fusion.1.refs_1_), channel_id=1, source_target_pairs={{0,1},{1,0},{2,3},{3,2},{4,5},{5,4},{6,7},{7,6},{8,9},{9,8},{10,11... | collective-permute-start | bytes 835592 | tf_op jit(solution)/shard_map/ppermute | solution.py:104
  27.3 2.0 %copy-start.2 = (bf16[2,32,2176]{2,1,0:T(8,128)(2,1)}, bf16[2,32,2176]{2,1,0:T(8,128)(2,1)S(1)}, u32[]{:S(2)}) copy-start(bf16[2,32,2176]{2,1,0:T(8,128)(2,1)S(1)} %pad_maximum_fusion.2.refs_2_) | copy-start | bytes 835588
  27.3 1.6 %collective-permute-start.9 = (bf16[2,32,2176]{2,1,0:T(8,128)(2,1)S(1)}, bf16[2,32,2176]{2,1,0:T(8,128)(2,1)S(1)}, u32[]{:S(2)}, u32[]{:S(2)}) collective-permute-start(bf16[2,32,2176]{2,1,0:T(8,128)(2,1)S(1)} %pad_maximum_fusion.2.refs_2_), channel_id=1, source_target_pairs={{0,1},{1,0},{2,3},{3,2},{4,5},{5,4},{6,7},{7,6},{8,9},{9,8},{10,11... | collective-permute-start | bytes 835592 | tf_op jit(solution)/shard_map/ppermute | solution.py:104
  27.4 1.9 %copy-start.3 = (bf16[2,32,2176]{2,1,0:T(8,128)(2,1)}, bf16[2,32,2176]{2,1,0:T(8,128)(2,1)S(1)}, u32[]{:S(2)}) copy-start(bf16[2,32,2176]{2,1,0:T(8,128)(2,1)S(1)} %pad_maximum_fusion.3.refs_3_) | copy-start | bytes 835588
  27.4 1.9 %collective-permute-start.10 = (bf16[2,32,2176]{2,1,0:T(8,128)(2,1)S(1)}, bf16[2,32,2176]{2,1,0:T(8,128)(2,1)S(1)}, u32[]{:S(2)}, u32[]{:S(2)}) collective-permute-start(bf16[2,32,2176]{2,1,0:T(8,128)(2,1)S(1)} %pad_maximum_fusion.3.refs_3_), channel_id=1, source_target_pairs={{0,1},{1,0},{2,3},{3,2},{4,5},{5,4},{6,7},{7,6},{8,9},{9,8},{10,11... | collective-permute-start | bytes 835592 | tf_op jit(solution)/shard_map/ppermute | solution.py:104
  28.0 1.4 %copy-start.4 = (bf16[2,32,2176]{2,1,0:T(8,128)(2,1)}, bf16[2,32,2176]{2,1,0:T(8,128)(2,1)S(1)}, u32[]{:S(2)}) copy-start(bf16[2,32,2176]{2,1,0:T(8,128)(2,1)S(1)} %collective-permute-done.7.refs_4_) | copy-start | bytes 835588
  28.0 1.4 %copy-start.5 = (bf16[2,32,2176]{2,1,0:T(8,128)(2,1)}, bf16[2,32,2176]{2,1,0:T(8,128)(2,1)S(1)}, u32[]{:S(2)}) copy-start(bf16[2,32,2176]{2,1,0:T(8,128)(2,1)S(1)} %collective-permute-done.8.refs_5_) | copy-start | bytes 835588
  28.9 0.7 copy-start.6
  29.3 0.7 copy-start.7
  38.7 6.1 %copy-start.9 = (bf16[2,512,128]{2,1,0:T(8,128)(2,1)S(1)}, bf16[2,512,128]{2,1,0:T(8,128)(2,1)}, u32[]{:S(2)}) copy-start(bf16[2,512,128]{2,1,0:T(8,128)(2,1)} %get-tuple-element.17) | copy-start | bytes 786436
  38.7 7.9 %copy-start.8 = (bf16[2,512,128]{2,1,0:T(8,128)(2,1)S(1)}, bf16[2,512,128]{2,1,0:T(8,128)(2,1)}, u32[]{:S(2)}) copy-start(bf16[2,512,128]{2,1,0:T(8,128)(2,1)} %get-tuple-element.19) | copy-start | bytes 786436
  38.7 1.8 %collective-permute-start.11 = (bf16[2,512,128]{2,1,0:T(8,128)(2,1)}, bf16[2,512,128]{2,1,0:T(8,128)(2,1)S(1)}, u32[]{:S(2)}, u32[]{:S(2)}) collective-permute-start(bf16[2,512,128]{2,1,0:T(8,128)(2,1)} %get-tuple-element.14), channel_id=1, source_target_pairs={{0,1},{1,0},{2,3},{3,2},{4,5},{5,4},{6,7},{7,6},{8,9},{9,8},{10,11... | collective-permute-start | bytes 786440 | tf_op jit(solution)/shard_map/ppermute | solution.py:104
  39.0 4.3 %collective-permute-start.13 = (bf16[2,512,128]{2,1,0:T(8,128)(2,1)}, bf16[2,512,128]{2,1,0:T(8,128)(2,1)S(1)}, u32[]{:S(2)}, u32[]{:S(2)}) collective-permute-start(bf16[2,512,128]{2,1,0:T(8,128)(2,1)} %get-tuple-element.16), channel_id=1, source_target_pairs={{0,1},{1,0},{2,3},{3,2},{4,5},{5,4},{6,7},{7,6},{8,9},{9,8},{10,11... | collective-permute-start | bytes 786440 | tf_op jit(solution)/shard_map/ppermute | solution.py:104
  39.3 5.5 %collective-permute-start.16 = (bf16[2,512,128]{2,1,0:T(8,128)(2,1)}, bf16[2,512,128]{2,1,0:T(8,128)(2,1)S(1)}, u32[]{:S(2)}, u32[]{:S(2)}) collective-permute-start(bf16[2,512,128]{2,1,0:T(8,128)(2,1)} %get-tuple-element.18), channel_id=1, source_target_pairs={{0,1},{1,0},{2,3},{3,2},{4,5},{5,4},{6,7},{7,6},{8,9},{9,8},{10,11... | collective-permute-start | bytes 786440 | tf_op jit(solution)/shard_map/ppermute | solution.py:104
  39.5 7.1 %collective-permute-start.19 = (bf16[2,512,128]{2,1,0:T(8,128)(2,1)}, bf16[2,512,128]{2,1,0:T(8,128)(2,1)S(1)}, u32[]{:S(2)}, u32[]{:S(2)}) collective-permute-start(bf16[2,512,128]{2,1,0:T(8,128)(2,1)} %get-tuple-element.20), channel_id=1, source_target_pairs={{0,1},{1,0},{2,3},{3,2},{4,5},{5,4},{6,7},{7,6},{8,9},{9,8},{10,11... | collective-permute-start | bytes 786440 | tf_op jit(solution)/shard_map/ppermute | solution.py:104
  41.6 18.0 %collective-permute-start.12 = (bf16[512,128]{1,0:T(8,128)(2,1)S(1)}, bf16[512,128]{1,0:T(8,128)(2,1)S(1)}, u32[]{:S(2)}, u32[]{:S(2)}) collective-permute-start(bf16[512,128]{1,0:T(8,128)(2,1)S(1)} %slice_bitcast_fusion.6), channel_id=1, source_target_pairs={{0,2},{1,3},{2,0},{3,1},{4,6},{5,7},{6,4},{7,5},{8,10},{9,11},{10,... | collective-permute-start | bytes 393224 | tf_op jit(solution)/shard_map/ppermute | solution.py:104
  44.4 34.4 %copy-start.10 = (f32[128]{0:T(128)S(1)}, f32[128]{0:T(128)}, u32[]{:S(2)}) copy-start(f32[128]{0:T(128)} %param.17) | copy-start | bytes 1540
  44.4 6.4 %collective-permute-start.14 = (bf16[512,128]{1,0:T(8,128)(2,1)S(1)}, bf16[512,128]{1,0:T(8,128)(2,1)S(1)}, u32[]{:S(2)}, u32[]{:S(2)}) collective-permute-start(bf16[512,128]{1,0:T(8,128)(2,1)S(1)} %slice_bitcast_fusion.4), channel_id=1, source_target_pairs={{0,2},{1,3},{2,0},{3,1},{4,6},{5,7},{6,4},{7,5},{8,10},{9,11},{10,... | collective-permute-start | bytes 393224 | tf_op jit(solution)/shard_map/ppermute | solution.py:104
  44.9 10.7 %collective-permute-start.17 = (bf16[512,128]{1,0:T(8,128)(2,1)S(1)}, bf16[512,128]{1,0:T(8,128)(2,1)S(1)}, u32[]{:S(2)}, u32[]{:S(2)}) collective-permute-start(bf16[512,128]{1,0:T(8,128)(2,1)S(1)} %slice_bitcast_fusion.2), channel_id=1, source_target_pairs={{0,2},{1,3},{2,0},{3,1},{4,6},{5,7},{6,4},{7,5},{8,10},{9,11},{10,... | collective-permute-start | bytes 393224 | tf_op jit(solution)/shard_map/ppermute | solution.py:104
  46.7 9.7 %collective-permute-start.20 = (bf16[512,128]{1,0:T(8,128)(2,1)S(1)}, bf16[512,128]{1,0:T(8,128)(2,1)S(1)}, u32[]{:S(2)}, u32[]{:S(2)}) collective-permute-start(bf16[512,128]{1,0:T(8,128)(2,1)S(1)} %slice_bitcast_fusion), channel_id=1, source_target_pairs={{0,2},{1,3},{2,0},{3,1},{4,6},{5,7},{6,4},{7,5},{8,10},{9,11},{10,... | collective-permute-start | bytes 393224 | tf_op jit(solution)/shard_map/ppermute | solution.py:104
  50.9 13.3 %collective-permute-start.15 = (bf16[512,128]{1,0:T(8,128)(2,1)S(1)}, bf16[512,128]{1,0:T(8,128)(2,1)S(1)}, u32[]{:S(2)}, u32[]{:S(2)}) collective-permute-start(bf16[512,128]{1,0:T(8,128)(2,1)S(1)} %fusion.2), channel_id=1, source_target_pairs={{0,8},{1,9},{2,10},{3,11},{4,12},{5,13},{6,14},{7,15},{8,0},{9,1},... | collective-permute-start | bytes 393224 | tf_op jit(solution)/shard_map/ppermute | solution.py:108
  55.6 8.6 %collective-permute-start.18 = (bf16[512,128]{1,0:T(8,128)(2,1)S(1)}, bf16[512,128]{1,0:T(8,128)(2,1)S(1)}, u32[]{:S(2)}, u32[]{:S(2)}) collective-permute-start(bf16[512,128]{1,0:T(8,128)(2,1)S(1)} %fusion.1), channel_id=1, source_target_pairs={{0,4},{1,5},{2,6},{3,7},{4,8},{5,9},{6,10},{7,11},{8,12},{9,13},{1... | collective-permute-start | bytes 393224 | tf_op jit(solution)/shard_map/ppermute | solution.py:108
  56.4 9.4 %collective-permute-start.21 = (bf16[512,128]{1,0:T(8,128)(2,1)S(1)}, bf16[512,128]{1,0:T(8,128)(2,1)S(1)}, u32[]{:S(2)}, u32[]{:S(2)}) collective-permute-start(bf16[512,128]{1,0:T(8,128)(2,1)S(1)} %fusion), channel_id=1, source_target_pairs={{0,12},{1,13},{2,14},{3,15},{4,0},{5,1},{6,2},{7,3},{8,4},{9,5},{1... | collective-permute-start | bytes 393224 | tf_op jit(solution)/shard_map/ppermute | solution.py:108
  66.0 1.2 %collective-permute-start.22 = (f32[512]{0:T(512)S(1)}, f32[512]{0:T(512)S(1)}, u32[]{:S(2)}, u32[]{:S(2)}) collective-permute-start(f32[512]{0:T(512)S(1)} %multiply_reduce_fusion), channel_id=1, source_target_pairs={{0,1},{1,0},{2,3},{3,2},{4,5},{5,4},{6,7},{7,6},{8,9},{9,8},{10,11... | collective-permute-start | bytes 6152 | tf_op jit(solution)/shard_map/ppermute | solution.py:104
  67.3 3.6 %collective-permute-start.23 = (f32[512]{0:T(512)S(1)}, f32[512]{0:T(512)S(1)}, u32[]{:S(2)}, u32[]{:S(2)}) collective-permute-start(f32[512]{0:T(512)S(1)} %add.65), channel_id=1, source_target_pairs={{0,2},{1,3},{2,0},{3,1},{4,6},{5,7},{6,4},{7,5},{8,10},{9,11},{10,... | collective-permute-start | bytes 6152 | tf_op jit(solution)/shard_map/ppermute | solution.py:104
  70.9 3.6 %collective-permute-start.26 = (f32[512]{0:T(512)S(1)}, f32[512]{0:T(512)S(1)}, u32[]{:S(2)}, u32[]{:S(2)}) collective-permute-start(f32[512]{0:T(512)S(1)} %add.66), channel_id=1, source_target_pairs={{0,12},{1,13},{2,14},{3,15},{4,0},{5,1},{6,2},{7,3},{8,4},{9,5},{1... | collective-permute-start | bytes 6152 | tf_op jit(solution)/shard_map/ppermute | solution.py:108
  72.2 4.5 %collective-permute-start.25 = (f32[512]{0:T(512)S(1)}, f32[512]{0:T(512)S(1)}, u32[]{:S(2)}, u32[]{:S(2)}) collective-permute-start(f32[512]{0:T(512)S(1)} %add.66), channel_id=1, source_target_pairs={{0,8},{1,9},{2,10},{3,11},{4,12},{5,13},{6,14},{7,15},{8,0},{9,1},... | collective-permute-start | bytes 6152 | tf_op jit(solution)/shard_map/ppermute | solution.py:108
  73.3 5.4 %collective-permute-start.24 = (f32[512]{0:T(512)S(1)}, f32[512]{0:T(512)S(1)}, u32[]{:S(2)}, u32[]{:S(2)}) collective-permute-start(f32[512]{0:T(512)S(1)} %add.66), channel_id=1, source_target_pairs={{0,4},{1,5},{2,6},{3,7},{4,8},{5,9},{6,10},{7,11},{8,12},{9,13},{1... | collective-permute-start | bytes 6152 | tf_op jit(solution)/shard_map/ppermute | solution.py:108

commit v2 on v1

--- a/solution.py
+++ b/solution.py
@@ -5,11 +5,13 @@
 from jax.experimental.pallas import tpu as pltpu
 from jax.sharding import PartitionSpec as P
 
+
 EPSILON = 1e-06
 LANES = 128
 F32 = jnp.float32
 BF16 = jnp.bfloat16
 NT = (((1,), (1,)), ((), ()))
+TN = (((0,), (0,)), ((), ()))
 
 
 def whole(count, memory=pltpu.VMEM):
@@ -24,39 +26,45 @@
     out[:, :width] = normed
     wide = normed.astype(F32)
     dot = lambda router: lax.dot_general(
-        wide, router[...], NT, precision=lax.Precision.HIGHEST, preferred_element_type=F32
+        router[...], wide, NT, precision=lax.Precision.HIGHEST, preferred_element_type=F32
     )
     group_exp = jnp.exp(dot(group_t))
     expert_exp = jnp.exp(dot(expert_t))
-    groups, experts = group_exp.shape[1], expert_exp.shape[1]
-    group_prob = group_exp / jnp.sum(group_exp, axis=1, keepdims=True)
-    lane = lax.broadcasted_iota(jnp.int32, expert_exp.shape, 1)
+    groups, experts = group_exp.shape[0], expert_exp.shape[0]
+    group_prob = group_exp / jnp.sum(group_exp, axis=0, keepdims=True)
+    lane = lax.broadcasted_iota(jnp.int32, expert_exp.shape, 0)
     chosen = jnp.zeros(expert_exp.shape, F32)
-    for slot in range(routes.shape[1]):
-        chosen = jnp.where(routes[:, slot : slot + 1] == lane, expert_exp, chosen)
+    for slot in range(routes.shape[0]):
+        chosen = jnp.where(routes[slot : slot + 1, :] == lane, expert_exp, chosen)
     spread = jnp.zeros(expert_exp.shape, F32)
     for group in range(groups):
         spread = jnp.where(
-            lane // (experts // groups) == group, group_prob[:, group : group + 1], spread
+            lane // (experts // groups) == group, group_prob[group : group + 1, :], spread
         )
-    weight = spread * (chosen / jnp.sum(chosen, axis=1, keepdims=True))
+    weight = spread * (chosen / jnp.sum(chosen, axis=0, keepdims=True))
     high = weight.astype(BF16)
     low = (weight - high.astype(F32)).astype(BF16)
     extra = out.shape[1] - width
     row = lax.broadcasted_iota(jnp.int32, (experts, extra), 0)
     column = lax.broadcasted_iota(jnp.int32, (experts, extra), 1)
-    place = lambda shift: jnp.where(column == row + shift, 1.0, 0.0).astype(BF16)
-    ext = jnp.dot(high, place(0), preferred_element_type=F32)
-    ext = ext + jnp.dot(low, place(experts), preferred_element_type=F32)
+    place = lambda move: jnp.where(column == row + move, 1.0, 0.0).astype(BF16)
+    spot = lambda part, move: lax.dot_general(
+        part, place(move), TN, preferred_element_type=F32
+    )
+    ext = spot(high, 0) + spot(low, experts)
     out[:, width:] = ext.astype(BF16)
 
 
 def expert_body(far, width, experts, block):
     def kernel(where_at, *refs):
         near_refs, peer_refs = refs[:far], refs[far : 2 * far]
-        w_gate, w_up, w_down = refs[2 * far : 2 * far + 3]
+        w_gate, up_far, down_far = refs[2 * far : 2 * far + 3]
         keep, send = refs[2 * far + 3 : 3 * far + 3], refs[3 * far + 3 : 4 * far + 3]
-        rows, result = refs[4 * far + 3], refs[4 * far + 4]
+        rows, result, w_up, w_down, up_done, down_done = refs[4 * far + 3 :]
+        up_copy = pltpu.make_async_copy(up_far, w_up, up_done)
+        down_copy = pltpu.make_async_copy(down_far, w_down, down_done)
+        up_copy.start()
+        down_copy.start()
         mine = where_at[0]
         top, mid, low = mine // 4, (mine // 2) % 2, mine % 2
         tok = near_refs[0].shape[1]
@@ -72,8 +80,10 @@
         weight = jnp.sum(jnp.where(hit, ext, 0.0), axis=1, keepdims=True)
         data = rows[:, :width]
         gate = jnp.dot(data, w_gate[0], preferred_element_type=F32)
+        up_copy.wait()
         upward = jnp.dot(data, w_up[0], preferred_element_type=F32)
         hidden = (gate / (1.0 + jnp.exp(-gate)) * upward * weight).astype(BF16)
+        down_copy.wait()
         result[...] = jnp.dot(hidden, w_down[0], preferred_element_type=F32).astype(BF16)
         for q in range(far):
             for s in range(2):
@@ -88,6 +98,10 @@
 
 def add(one, two):
     return (one.astype(F32) + two.astype(F32)).astype(BF16)
+
+
+def far_order(far):
+    return sorted(range(1, far), key=lambda q: -min(q, far - q))
 
 
 def per_device(
@@ -109,12 +123,12 @@
 
     payload = pl.pallas_call(
         payload_kernel,
-        out_shape=jax.ShapeDtypeStruct((tok, width + extra), BF16),
+        out_shape=pltpu.VMEM((tok, width + extra), BF16),
         in_specs=whole(5),
         out_specs=pl.BlockSpec(memory_space=pltpu.VMEM),
-    )(tokens, routes, in_gain[None, :], group_router.T, expert_router.T)
+    )(tokens, routes.T, in_gain[None, :], group_router.T, expert_router.T)
 
-    steps = [1, far - 1] + [q for q in range(2, far - 1)]
+    steps = far_order(far)
     held = {0: payload}
     for q in steps:
         held[q] = shift(payload, q)
@@ -123,26 +137,32 @@
         near[q] = jnp.stack([held[q], flip(held[q], 2)])
         peer[q] = flip(near[q], 1)
     total = ep * tok
-    piece = jax.ShapeDtypeStruct((2, total, block), BF16)
+    piece = pltpu.VMEM((2, total, block), BF16)
+    local = lambda value: pltpu.with_memory_space_constraint(value, pltpu.VMEM)
     parts = pl.pallas_call(
         expert_body(far, width, experts, block),
         out_shape=[piece] * (2 * far),
-        in_specs=whole(1, pltpu.SMEM) + whole(2 * far + 3),
+        in_specs=whole(1, pltpu.SMEM) + whole(2 * far + 1) + whole(2, pltpu.HBM),
         out_specs=whole(2 * far),
         scratch_shapes=[
             pltpu.VMEM((total, width + extra), BF16),
             pltpu.VMEM((total, width), BF16),
+            pltpu.VMEM(w_up.shape, BF16),
+            pltpu.VMEM(w_down.shape, BF16),
+            pltpu.SemaphoreType.DMA,
+            pltpu.SemaphoreType.DMA,
         ],
+        compiler_params=pltpu.CompilerParams(vmem_limit_bytes=28 << 20),
     )(
         mine[None],
-        *[near[q] for q in range(far)],
-        *[peer[q] for q in range(far)],
-        w_gate,
-        w_up,
-        w_down,
+        *[local(near[q]) for q in range(far)],
+        *[local(peer[q]) for q in range(far)],
+        local(w_gate),
+        pltpu.with_memory_space_constraint(w_up, pltpu.HBM),
+        pltpu.with_memory_space_constraint(w_down, pltpu.HBM),
     )
     keep, send = parts[:far], parts[far:]
-    order = [q for q in range(2, far - 1)] + [1, far - 1, 0]
+    order = steps + [0]
     landed = {}
     for q in order:
         paired = add(keep[q], flip(send[q], 1))

time: 79.8 us -> 73.2 us (0.917)
  other arithmetic: 4.32 us -> 1.51 us
  Pallas kernels: 11.4 us -> 9.11 us
  local copies, waits for them, and re-layouts: 2.11 us -> 0.05 us
  starting transfers between devices: 30.5 us -> 31.3 us
    unnamed x23 -> x4, local copies, waits for them, and re-layouts: 2.07 us -> 0.01 us
    convert_element_type x7, other arithmetic: 2.3 us -> 0.4 us  [add(): return (one.astype(F32) + two.astype(F32)).astype(BF16)]
    pallas_call x1, Pallas kernels: 8.7 us -> 7.12 us  [per_device(): pl.pallas_call(expert_body(far, width, experts, block), out_shape=[piece]...]
    ppermute x18, starting transfers between devices: 13 us -> 14.4 us  [flip(): return lax.ppermute(value, 'ep', [(i, i ^ bit) for i in range(ep)])]
    another operation x4, other arithmetic: 1.04 us -> 0.13 us  [per_device(): near[q] = jnp.stack([held[q], flip(held[q], 2)])]
  transfers between devices with their start and end apart: 27 -> 27, of which waited for: 14 -> 16; matrix products, arithmetic and copies ran while one was open for 4% -> 1% of each run, Pallas kernels for 0% -> 0%
where the time goes in v2:
time: 73.2 us; the launch traced here: 73.1 us
  starting transfers between devices  31.3 us (43%)
  waiting for transfers between devices  30.9 us (42%)
  Pallas kernels  9.11 us (12%)
  other arithmetic  1.51 us (2%)
    ppermute x9, waiting for transfers between devices, shift(): return lax.ppermute(value, 'ep', moves)  17.2 us
    ppermute x9, starting transfers between devices, shift(): return lax.ppermute(value, 'ep', moves)  16.9 us
    ppermute x18, starting transfers between devices, flip(): return lax.ppermute(value, 'ep', [(i, i ^ bit) for i in range(ep)])  14.4 us
    ppermute x18, waiting for transfers between devices, flip(): return lax.ppermute(value, 'ep', [(i, i ^ bit) for i in range(ep)])  13.7 us
    pallas_call x1, Pallas kernels, per_device(): pl.pallas_call(expert_body(far, width, experts, block), out_shape=[piece]...  7.12 us
    pallas_call x1, Pallas kernels, per_device(): pl.pallas_call(payload_kernel, out_shape=pltpu.VMEM((tok, width + extra),...  1.99 us
  transfers between devices with their start and end apart: 27, of which 16 were waited for; matrix products, arithmetic and copies ran while one was open for 1% of the time, Pallas kernels for 0%

profile of v2, /device:TPU:0, one launch (start us, length us, event | category | flops | bytes accessed | tf_op | source)
XLA Modules:
  0.0 73.1 jit_solution(4004157609886534561)
XLA Ops:
  0.0 2.0 %shard_map.91 = bf16[32,2176]{1,0:T(8,128)(2,1)S(1)} custom-call(bf16[32,2048]{1,0:T(8,128)(2,1)} %tokens.1, s32[4,32]{1,0:T(4,128)} %bitcast.56, f32[1,2048]{1,0:T(1,128)} %bitcast.55, f32[4,2048]{1,0:T(4,128)} %bitcast.54, f32[16,2048]{1,0:T(8,128)} %bitcast.53), custom_call_target="tpu_custom_call" | custom-call | tf_op jit(solution)/shard_map/pallas_call | solution.py:124
  2.0 3.1 %collective-permute-start.1 = (bf16[32,2176]{1,0:T(8,128)(2,1)S(1)}, bf16[32,2176]{1,0:T(8,128)(2,1)S(1)}, u32[]{:S(2)}, u32[]{:S(2)}) collective-permute-start(bf16[32,2176]{1,0:T(8,128)(2,1)S(1)} %shard_map.91), channel_id=1, source_target_pairs={{0,4},{1,5},{2,6},{3,7},{4,8},{5,9},{6,10},{7,11},{8,12},{9,13},{1... | collective-permute-start | bytes 417800 | tf_op jit(solution)/shard_map/ppermute | solution.py:122
  5.1 1.5 %collective-permute-start = (bf16[32,2176]{1,0:T(8,128)(2,1)S(1)}, bf16[32,2176]{1,0:T(8,128)(2,1)S(1)}, u32[]{:S(2)}, u32[]{:S(2)}) collective-permute-start(bf16[32,2176]{1,0:T(8,128)(2,1)S(1)} %shard_map.91), channel_id=1, source_target_pairs={{0,2},{1,3},{2,0},{3,1},{4,6},{5,7},{6,4},{7,5},{8,10},{9,11},{10,... | collective-permute-start | bytes 417800 | tf_op jit(solution)/shard_map/ppermute | solution.py:118
  6.6 2.2 %collective-permute-start.5 = (bf16[32,2176]{1,0:T(8,128)(2,1)S(1)}, bf16[32,2176]{1,0:T(8,128)(2,1)S(1)}, u32[]{:S(2)}, u32[]{:S(2)}) collective-permute-start(bf16[32,2176]{1,0:T(8,128)(2,1)S(1)} %shard_map.91), channel_id=1, source_target_pairs={{0,12},{1,13},{2,14},{3,15},{4,0},{5,1},{6,2},{7,3},{8,4},{9,5},{1... | collective-permute-start | bytes 417800 | tf_op jit(solution)/shard_map/ppermute | solution.py:122
  8.8 0.8 %collective-permute-start.3 = (bf16[32,2176]{1,0:T(8,128)(2,1)S(1)}, bf16[32,2176]{1,0:T(8,128)(2,1)S(1)}, u32[]{:S(2)}, u32[]{:S(2)}) collective-permute-start(bf16[32,2176]{1,0:T(8,128)(2,1)S(1)} %shard_map.91), channel_id=1, source_target_pairs={{0,8},{1,9},{2,10},{3,11},{4,12},{5,13},{6,14},{7,15},{8,0},{9,1},... | collective-permute-start | bytes 417800 | tf_op jit(solution)/shard_map/ppermute | solution.py:122
  9.6 1.4 %collective-permute-done.1 = bf16[32,2176]{1,0:T(8,128)(2,1)S(1)} collective-permute-done((bf16[32,2176]{1,0:T(8,128)(2,1)S(1)}, bf16[32,2176]{1,0:T(8,128)(2,1)S(1)}, u32[]{:S(2)}, u32[]{:S(2)}) %collective-permute-start.1) | collective-permute-done | bytes 139296 | tf_op jit(solution)/shard_map/ppermute | solution.py:122
  11.0 2.3 %collective-permute-start.2 = (bf16[32,2176]{1,0:T(8,128)(2,1)S(1)}, bf16[32,2176]{1,0:T(8,128)(2,1)S(1)}, u32[]{:S(2)}, u32[]{:S(2)}) collective-permute-start(bf16[32,2176]{1,0:T(8,128)(2,1)S(1)} %collective-permute-done.1), channel_id=1, source_target_pairs={{0,2},{1,3},{2,0},{3,1},{4,6},{5,7},{6,4},{7,5},{8,10},{9,11},{10,... | collective-permute-start | bytes 417800 | tf_op jit(solution)/shard_map/ppermute | solution.py:118
  13.3 0.0 collective-permute-done
  13.4 0.1 collective-permute-start.7
  13.5 0.3 collective-permute-done.5
  13.7 1.2 %collective-permute-start.6 = (bf16[32,2176]{1,0:T(8,128)(2,1)S(1)}, bf16[32,2176]{1,0:T(8,128)(2,1)S(1)}, u32[]{:S(2)}, u32[]{:S(2)}) collective-permute-start(bf16[32,2176]{1,0:T(8,128)(2,1)S(1)} %collective-permute-done.5), channel_id=1, source_target_pairs={{0,2},{1,3},{2,0},{3,1},{4,6},{5,7},{6,4},{7,5},{8,10},{9,11},{10,... | collective-permute-start | bytes 417800 | tf_op jit(solution)/shard_map/ppermute | solution.py:118
  14.9 4.8 %collective-permute-done.3 = bf16[32,2176]{1,0:T(8,128)(2,1)S(1)} collective-permute-done((bf16[32,2176]{1,0:T(8,128)(2,1)S(1)}, bf16[32,2176]{1,0:T(8,128)(2,1)S(1)}, u32[]{:S(2)}, u32[]{:S(2)}) %collective-permute-start.3) | collective-permute-done | bytes 139296 | tf_op jit(solution)/shard_map/ppermute | solution.py:122
  19.7 1.5 %collective-permute-start.4 = (bf16[32,2176]{1,0:T(8,128)(2,1)S(1)}, bf16[32,2176]{1,0:T(8,128)(2,1)S(1)}, u32[]{:S(2)}, u32[]{:S(2)}) collective-permute-start(bf16[32,2176]{1,0:T(8,128)(2,1)S(1)} %collective-permute-done.3), channel_id=1, source_target_pairs={{0,2},{1,3},{2,0},{3,1},{4,6},{5,7},{6,4},{7,5},{8,10},{9,11},{10,... | collective-permute-start | bytes 417800 | tf_op jit(solution)/shard_map/ppermute | solution.py:118
  21.2 0.0 collective-permute-done.2
  21.3 0.1 collective-permute-start.8
  21.3 3.6 %collective-permute-done.4 = bf16[32,2176]{1,0:T(8,128)(2,1)S(1)} collective-permute-done((bf16[32,2176]{1,0:T(8,128)(2,1)S(1)}, bf16[32,2176]{1,0:T(8,128)(2,1)S(1)}, u32[]{:S(2)}, u32[]{:S(2)}) %collective-permute-start.4) | collective-permute-done | bytes 139296 | tf_op jit(solution)/shard_map/ppermute | solution.py:118
  25.0 0.1 collective-permute-start.9
  25.1 0.0 collective-permute-done.6
  25.2 0.5 collective-permute-start.10
  25.7 0.0 collective-permute-done.7.refs_4_
  25.7 0.0 collective-permute-done.8.refs_5_
  25.7 1.1 %collective-permute-done.9.refs_6_ = bf16[2,32,2176]{2,1,0:T(8,128)(2,1)} collective-permute-done((bf16[2,32,2176]{2,1,0:T(8,128)(2,1)S(1)}, bf16[2,32,2176]{2,1,0:T(8,128)(2,1)}, u32[]{:S(2)}, u32[]{:S(2)}) %collective-permute-start.9) | collective-permute-done | bytes 278560 | tf_op jit(solution)/shard_map/ppermute | solution.py:118
  26.8 0.4 collective-permute-done.10.refs_7_
  27.2 0.0 copy-done
  27.2 7.1 %shard_map.92 = (bf16[2,512,128]{2,1,0:T(8,128)(2,1)S(1)}, bf16[2,512,128]{2,1,0:T(8,128)(2,1)S(1)}, bf16[2,512,128]{2,1,0:T(8,128)(2,1)S(1)}, bf16[2,512,128]{2...) custom-call(s32[1]{0:T(128)} %bitcast.where_at, ...), custom_call_target="tpu_custom_call" | custom-call | tf_op jit(solution)/shard_map/pallas_call | solution.py:142
  34.3 0.3 collective-permute-start.11
  34.6 0.3 collective-permute-start.13
  34.9 0.2 collective-permute-start.16
  35.1 0.3 collective-permute-start.19
  35.4 0.5 collective-permute-done.11
  35.9 0.1 add_convert_fusion.3
  36.0 1.8 %collective-permute-start.12 = (bf16[512,128]{1,0:T(8,128)(2,1)S(1)}, bf16[512,128]{1,0:T(8,128)(2,1)S(1)}, u32[]{:S(2)}, u32[]{:S(2)}) collective-permute-start(bf16[512,128]{1,0:T(8,128)(2,1)S(1)} %slice_bitcast_fusion.6), channel_id=1, source_target_pairs={{0,2},{1,3},{2,0},{3,1},{4,6},{5,7},{6,4},{7,5},{8,10},{9,11},{10,... | collective-permute-start | bytes 393224 | tf_op jit(solution)/shard_map/ppermute | solution.py:118
  37.8 0.0 collective-permute-done.13
  37.8 0.1 add_convert_fusion.2
  37.8 0.0 copy-start.1
  37.9 0.4 collective-permute-start.14
  38.3 0.0 collective-permute-done.16
  38.3 0.1 add_convert_fusion.1
  38.4 1.8 %collective-permute-start.17 = (bf16[512,128]{1,0:T(8,128)(2,1)S(1)}, bf16[512,128]{1,0:T(8,128)(2,1)S(1)}, u32[]{:S(2)}, u32[]{:S(2)}) collective-permute-start(bf16[512,128]{1,0:T(8,128)(2,1)S(1)} %slice_bitcast_fusion.2), channel_id=1, source_target_pairs={{0,2},{1,3},{2,0},{3,1},{4,6},{5,7},{6,4},{7,5},{8,10},{9,11},{10,... | collective-permute-start | bytes 393224 | tf_op jit(solution)/shard_map/ppermute | solution.py:118
  40.1 0.0 collective-permute-done.19
  40.1 0.1 add_convert_fusion
  40.2 0.4 collective-permute-start.20
  40.6 4.6 %collective-permute-done.14 = bf16[512,128]{1,0:T(8,128)(2,1)S(1)} collective-permute-done((bf16[512,128]{1,0:T(8,128)(2,1)S(1)}, bf16[512,128]{1,0:T(8,128)(2,1)S(1)}, u32[]{:S(2)}, u32[]{:S(2)}) %collective-permute-start.14) | collective-permute-done | bytes 131104 | tf_op jit(solution)/shard_map/ppermute | solution.py:118
  45.3 3.7 %collective-permute-start.15 = (bf16[512,128]{1,0:T(8,128)(2,1)S(1)}, bf16[512,128]{1,0:T(8,128)(2,1)S(1)}, u32[]{:S(2)}, u32[]{:S(2)}) collective-permute-start(bf16[512,128]{1,0:T(8,128)(2,1)S(1)} %fusion.2), channel_id=1, source_target_pairs={{0,8},{1,9},{2,10},{3,11},{4,12},{5,13},{6,14},{7,15},{8,0},{9,1},... | collective-permute-start | bytes 393224 | tf_op jit(solution)/shard_map/ppermute | solution.py:122
  49.0 0.0 collective-permute-done.17
  49.1 0.7 collective-permute-start.18
  49.8 0.3 collective-permute-done.20
  50.2 2.9 %collective-permute-start.21 = (bf16[512,128]{1,0:T(8,128)(2,1)S(1)}, bf16[512,128]{1,0:T(8,128)(2,1)S(1)}, u32[]{:S(2)}, u32[]{:S(2)}) collective-permute-start(bf16[512,128]{1,0:T(8,128)(2,1)S(1)} %fusion), channel_id=1, source_target_pairs={{0,12},{1,13},{2,14},{3,15},{4,0},{5,1},{6,2},{7,3},{8,4},{9,5},{1... | collective-permute-start | bytes 393224 | tf_op jit(solution)/shard_map/ppermute | solution.py:122
  53.1 0.0 collective-permute-done.12
  53.1 4.6 %collective-permute-done.15 = bf16[512,128]{1,0:T(8,128)(2,1)S(1)} collective-permute-done((bf16[512,128]{1,0:T(8,128)(2,1)S(1)}, bf16[512,128]{1,0:T(8,128)(2,1)S(1)}, u32[]{:S(2)}, u32[]{:S(2)}) %collective-permute-start.15) | collective-permute-done | bytes 131104 | tf_op jit(solution)/shard_map/ppermute | solution.py:122
  57.6 0.0 collective-permute-done.18
  57.6 1.9 %collective-permute-done.21 = bf16[512,128]{1,0:T(8,128)(2,1)S(1)} collective-permute-done((bf16[512,128]{1,0:T(8,128)(2,1)S(1)}, bf16[512,128]{1,0:T(8,128)(2,1)S(1)}, u32[]{:S(2)}, u32[]{:S(2)}) %collective-permute-start.21) | collective-permute-done | bytes 131104 | tf_op jit(solution)/shard_map/ppermute | solution.py:122
  59.5 0.2 multiply_reduce_fusion
  59.7 0.1 collective-permute-start.22
  59.7 1.1 %collective-permute-done.22 = f32[512]{0:T(512)S(1)} collective-permute-done((f32[512]{0:T(512)S(1)}, f32[512]{0:T(512)S(1)}, u32[]{:S(2)}, u32[]{:S(2)}) %collective-permute-start.22) | collective-permute-done | bytes 2080 | tf_op jit(solution)/shard_map/ppermute | solution.py:118
  60.9 1.6 %collective-permute-start.23 = (f32[512]{0:T(512)S(1)}, f32[512]{0:T(512)S(1)}, u32[]{:S(2)}, u32[]{:S(2)}) collective-permute-start(f32[512]{0:T(512)S(1)} %add.65), channel_id=1, source_target_pairs={{0,2},{1,3},{2,0},{3,1},{4,6},{5,7},{6,4},{7,5},{8,10},{9,11},{10,... | collective-permute-start | bytes 6152 | tf_op jit(solution)/shard_map/ppermute | solution.py:118
  62.5 1.9 %collective-permute-done.23 = f32[512]{0:T(512)S(1)} collective-permute-done((f32[512]{0:T(512)S(1)}, f32[512]{0:T(512)S(1)}, u32[]{:S(2)}, u32[]{:S(2)}) %collective-permute-start.23) | collective-permute-done | bytes 2080 | tf_op jit(solution)/shard_map/ppermute | solution.py:118
  64.5 1.1 %collective-permute-start.26 = (f32[512]{0:T(512)S(1)}, f32[512]{0:T(512)S(1)}, u32[]{:S(2)}, u32[]{:S(2)}) collective-permute-start(f32[512]{0:T(512)S(1)} %add.66), channel_id=1, source_target_pairs={{0,12},{1,13},{2,14},{3,15},{4,0},{5,1},{6,2},{7,3},{8,4},{9,5},{1... | collective-permute-start | bytes 6152 | tf_op jit(solution)/shard_map/ppermute | solution.py:122
  65.6 1.2 %collective-permute-start.25 = (f32[512]{0:T(512)S(1)}, f32[512]{0:T(512)S(1)}, u32[]{:S(2)}, u32[]{:S(2)}) collective-permute-start(f32[512]{0:T(512)S(1)} %add.66), channel_id=1, source_target_pairs={{0,8},{1,9},{2,10},{3,11},{4,12},{5,13},{6,14},{7,15},{8,0},{9,1},... | collective-permute-start | bytes 6152 | tf_op jit(solution)/shard_map/ppermute | solution.py:122
  66.9 1.1 %collective-permute-start.24 = (f32[512]{0:T(512)S(1)}, f32[512]{0:T(512)S(1)}, u32[]{:S(2)}, u32[]{:S(2)}) collective-permute-start(f32[512]{0:T(512)S(1)} %add.66), channel_id=1, source_target_pairs={{0,4},{1,5},{2,6},{3,7},{4,8},{5,9},{6,10},{7,11},{8,12},{9,13},{1... | collective-permute-start | bytes 6152 | tf_op jit(solution)/shard_map/ppermute | solution.py:122
  67.9 0.1 collective-permute-done.26
  68.1 2.0 %collective-permute-done.25 = f32[512]{0:T(512)S(1)} collective-permute-done((f32[512]{0:T(512)S(1)}, f32[512]{0:T(512)S(1)}, u32[]{:S(2)}, u32[]{:S(2)}) %collective-permute-start.25) | collective-permute-done | bytes 2080 | tf_op jit(solution)/shard_map/ppermute | solution.py:122
  70.1 2.1 %collective-permute-done.24 = f32[512]{0:T(512)S(1)} collective-permute-done((f32[512]{0:T(512)S(1)}, f32[512]{0:T(512)S(1)}, u32[]{:S(2)}, u32[]{:S(2)}) %collective-permute-start.24) | collective-permute-done | bytes 2080 | tf_op jit(solution)/shard_map/ppermute | solution.py:122
  72.3 0.8 %multiply_convert_fusion = bf16[512,128]{1,0:T(8,128)(2,1)} fusion(f32[128]{0:T(128)S(1)} %copy-done.1, f32[512]{0:T(512)S(1)} %add_rsqrt_fusion, bf16[512,128]{1,0:T(8,128)(2,1)S(1)} %collective-permute-done.21, bf16[512,128]{1,0:T(8,128)(2,1)S(1)} %collective-permute-done.18, bf16[512,128]{1,0:T(8,128)(2,1)S(1)} %collective-permute-done.15, ...), kind=kLoop, calls=%fused_computation.16 | loop fusion | flops 917504 | bytes 788992 | tf_op jit(solution)/shard_map/convert_element_type | solution.py:181
  (16 shorter events, 0.3 us)
Async XLA Ops:
  0.0 27.2 %copy-start = (bf16[1,2048,512]{2,1,0:T(8,128)(2,1)S(1)}, bf16[1,2048,512]{2,1,0:T(8,128)(2,1)}, u32[]{:S(2)}) copy-start(bf16[1,2048,512]{2,1,0:T(8,128)(2,1)} %refs_8_.1) | copy-start | bytes 6291460
  2.0 9.0 %collective-permute-start.1 = (bf16[32,2176]{1,0:T(8,128)(2,1)S(1)}, bf16[32,2176]{1,0:T(8,128)(2,1)S(1)}, u32[]{:S(2)}, u32[]{:S(2)}) collective-permute-start(bf16[32,2176]{1,0:T(8,128)(2,1)S(1)} %shard_map.91), channel_id=1, source_target_pairs={{0,4},{1,5},{2,6},{3,7},{4,8},{5,9},{6,10},{7,11},{8,12},{9,13},{1... | collective-permute-start | bytes 417800 | tf_op jit(solution)/shard_map/ppermute | solution.py:122
  5.1 8.3 %collective-permute-start = (bf16[32,2176]{1,0:T(8,128)(2,1)S(1)}, bf16[32,2176]{1,0:T(8,128)(2,1)S(1)}, u32[]{:S(2)}, u32[]{:S(2)}) collective-permute-start(bf16[32,2176]{1,0:T(8,128)(2,1)S(1)} %shard_map.91), channel_id=1, source_target_pairs={{0,2},{1,3},{2,0},{3,1},{4,6},{5,7},{6,4},{7,5},{8,10},{9,11},{10,... | collective-permute-start | bytes 417800 | tf_op jit(solution)/shard_map/ppermute | solution.py:118
  6.6 7.2 %collective-permute-start.5 = (bf16[32,2176]{1,0:T(8,128)(2,1)S(1)}, bf16[32,2176]{1,0:T(8,128)(2,1)S(1)}, u32[]{:S(2)}, u32[]{:S(2)}) collective-permute-start(bf16[32,2176]{1,0:T(8,128)(2,1)S(1)} %shard_map.91), channel_id=1, source_target_pairs={{0,12},{1,13},{2,14},{3,15},{4,0},{5,1},{6,2},{7,3},{8,4},{9,5},{1... | collective-permute-start | bytes 417800 | tf_op jit(solution)/shard_map/ppermute | solution.py:122
  8.8 10.9 %collective-permute-start.3 = (bf16[32,2176]{1,0:T(8,128)(2,1)S(1)}, bf16[32,2176]{1,0:T(8,128)(2,1)S(1)}, u32[]{:S(2)}, u32[]{:S(2)}) collective-permute-start(bf16[32,2176]{1,0:T(8,128)(2,1)S(1)} %shard_map.91), channel_id=1, source_target_pairs={{0,8},{1,9},{2,10},{3,11},{4,12},{5,13},{6,14},{7,15},{8,0},{9,1},... | collective-permute-start | bytes 417800 | tf_op jit(solution)/shard_map/ppermute | solution.py:122
  11.0 10.2 %collective-permute-start.2 = (bf16[32,2176]{1,0:T(8,128)(2,1)S(1)}, bf16[32,2176]{1,0:T(8,128)(2,1)S(1)}, u32[]{:S(2)}, u32[]{:S(2)}) collective-permute-start(bf16[32,2176]{1,0:T(8,128)(2,1)S(1)} %collective-permute-done.1), channel_id=1, source_target_pairs={{0,2},{1,3},{2,0},{3,1},{4,6},{5,7},{6,4},{7,5},{8,10},{9,11},{10,... | collective-permute-start | bytes 417800 | tf_op jit(solution)/shard_map/ppermute | solution.py:118
  13.4 12.3 %collective-permute-start.7 = (bf16[2,32,2176]{2,1,0:T(8,128)(2,1)S(1)}, bf16[2,32,2176]{2,1,0:T(8,128)(2,1)}, u32[]{:S(2)}, u32[]{:S(2)}) collective-permute-start(bf16[2,32,2176]{2,1,0:T(8,128)(2,1)S(1)} %pad_maximum_fusion.refs_0_), channel_id=1, source_target_pairs={{0,1},{1,0},{2,3},{3,2},{4,5},{5,4},{6,7},{7,6},{8,9},{9,8},{10,11... | collective-permute-start | bytes 835592 | tf_op jit(solution)/shard_map/ppermute | solution.py:118
  13.7 11.4 %collective-permute-start.6 = (bf16[32,2176]{1,0:T(8,128)(2,1)S(1)}, bf16[32,2176]{1,0:T(8,128)(2,1)S(1)}, u32[]{:S(2)}, u32[]{:S(2)}) collective-permute-start(bf16[32,2176]{1,0:T(8,128)(2,1)S(1)} %collective-permute-done.5), channel_id=1, source_target_pairs={{0,2},{1,3},{2,0},{3,1},{4,6},{5,7},{6,4},{7,5},{8,10},{9,11},{10,... | collective-permute-start | bytes 417800 | tf_op jit(solution)/shard_map/ppermute | solution.py:118
  19.7 5.3 %collective-permute-start.4 = (bf16[32,2176]{1,0:T(8,128)(2,1)S(1)}, bf16[32,2176]{1,0:T(8,128)(2,1)S(1)}, u32[]{:S(2)}, u32[]{:S(2)}) collective-permute-start(bf16[32,2176]{1,0:T(8,128)(2,1)S(1)} %collective-permute-done.3), channel_id=1, source_target_pairs={{0,2},{1,3},{2,0},{3,1},{4,6},{5,7},{6,4},{7,5},{8,10},{9,11},{10,... | collective-permute-start | bytes 417800 | tf_op jit(solution)/shard_map/ppermute | solution.py:118
  21.3 4.5 %collective-permute-start.8 = (bf16[2,32,2176]{2,1,0:T(8,128)(2,1)S(1)}, bf16[2,32,2176]{2,1,0:T(8,128)(2,1)}, u32[]{:S(2)}, u32[]{:S(2)}) collective-permute-start(bf16[2,32,2176]{2,1,0:T(8,128)(2,1)S(1)} %pad_maximum_fusion.1.refs_1_), channel_id=1, source_target_pairs={{0,1},{1,0},{2,3},{3,2},{4,5},{5,4},{6,7},{7,6},{8,9},{9,8},{10,11... | collective-permute-start | bytes 835592 | tf_op jit(solution)/shard_map/ppermute | solution.py:118
  25.0 1.8 %collective-permute-start.9 = (bf16[2,32,2176]{2,1,0:T(8,128)(2,1)S(1)}, bf16[2,32,2176]{2,1,0:T(8,128)(2,1)}, u32[]{:S(2)}, u32[]{:S(2)}) collective-permute-start(bf16[2,32,2176]{2,1,0:T(8,128)(2,1)S(1)} %pad_maximum_fusion.2.refs_2_), channel_id=1, source_target_pairs={{0,1},{1,0},{2,3},{3,2},{4,5},{5,4},{6,7},{7,6},{8,9},{9,8},{10,11... | collective-permute-start | bytes 835592 | tf_op jit(solution)/shard_map/ppermute | solution.py:118
  25.2 2.0 %collective-permute-start.10 = (bf16[2,32,2176]{2,1,0:T(8,128)(2,1)S(1)}, bf16[2,32,2176]{2,1,0:T(8,128)(2,1)}, u32[]{:S(2)}, u32[]{:S(2)}) collective-permute-start(bf16[2,32,2176]{2,1,0:T(8,128)(2,1)S(1)} %pad_maximum_fusion.3.refs_3_), channel_id=1, source_target_pairs={{0,1},{1,0},{2,3},{3,2},{4,5},{5,4},{6,7},{7,6},{8,9},{9,8},{10,11... | collective-permute-start | bytes 835592 | tf_op jit(solution)/shard_map/ppermute | solution.py:118
  34.3 1.6 %collective-permute-start.11 = (bf16[2,512,128]{2,1,0:T(8,128)(2,1)S(1)}, bf16[2,512,128]{2,1,0:T(8,128)(2,1)S(1)}, u32[]{:S(2)}, u32[]{:S(2)}) collective-permute-start(bf16[2,512,128]{2,1,0:T(8,128)(2,1)S(1)} %get-tuple-element.14), channel_id=1, source_target_pairs={{0,1},{1,0},{2,3},{3,2},{4,5},{5,4},{6,7},{7,6},{8,9},{9,8},{10,11... | collective-permute-start | bytes 786440 | tf_op jit(solution)/shard_map/ppermute | solution.py:118
  34.6 3.2 %collective-permute-start.13 = (bf16[2,512,128]{2,1,0:T(8,128)(2,1)S(1)}, bf16[2,512,128]{2,1,0:T(8,128)(2,1)S(1)}, u32[]{:S(2)}, u32[]{:S(2)}) collective-permute-start(bf16[2,512,128]{2,1,0:T(8,128)(2,1)S(1)} %get-tuple-element.16), channel_id=1, source_target_pairs={{0,1},{1,0},{2,3},{3,2},{4,5},{5,4},{6,7},{7,6},{8,9},{9,8},{10,11... | collective-permute-start | bytes 786440 | tf_op jit(solution)/shard_map/ppermute | solution.py:118
  34.9 3.4 %collective-permute-start.16 = (bf16[2,512,128]{2,1,0:T(8,128)(2,1)S(1)}, bf16[2,512,128]{2,1,0:T(8,128)(2,1)S(1)}, u32[]{:S(2)}, u32[]{:S(2)}) collective-permute-start(bf16[2,512,128]{2,1,0:T(8,128)(2,1)S(1)} %get-tuple-element.18), channel_id=1, source_target_pairs={{0,1},{1,0},{2,3},{3,2},{4,5},{5,4},{6,7},{7,6},{8,9},{9,8},{10,11... | collective-permute-start | bytes 786440 | tf_op jit(solution)/shard_map/ppermute | solution.py:118
  35.1 5.0 %collective-permute-start.19 = (bf16[2,512,128]{2,1,0:T(8,128)(2,1)S(1)}, bf16[2,512,128]{2,1,0:T(8,128)(2,1)S(1)}, u32[]{:S(2)}, u32[]{:S(2)}) collective-permute-start(bf16[2,512,128]{2,1,0:T(8,128)(2,1)S(1)} %get-tuple-element.20), channel_id=1, source_target_pairs={{0,1},{1,0},{2,3},{3,2},{4,5},{5,4},{6,7},{7,6},{8,9},{9,8},{10,11... | collective-permute-start | bytes 786440 | tf_op jit(solution)/shard_map/ppermute | solution.py:118
  36.0 17.1 %collective-permute-start.12 = (bf16[512,128]{1,0:T(8,128)(2,1)S(1)}, bf16[512,128]{1,0:T(8,128)(2,1)S(1)}, u32[]{:S(2)}, u32[]{:S(2)}) collective-permute-start(bf16[512,128]{1,0:T(8,128)(2,1)S(1)} %slice_bitcast_fusion.6), channel_id=1, source_target_pairs={{0,2},{1,3},{2,0},{3,1},{4,6},{5,7},{6,4},{7,5},{8,10},{9,11},{10,... | collective-permute-start | bytes 393224 | tf_op jit(solution)/shard_map/ppermute | solution.py:118
  37.8 34.4 %copy-start.1 = (f32[128]{0:T(128)S(1)}, f32[128]{0:T(128)}, u32[]{:S(2)}) copy-start(f32[128]{0:T(128)} %param.17) | copy-start | bytes 1540
  37.9 7.4 %collective-permute-start.14 = (bf16[512,128]{1,0:T(8,128)(2,1)S(1)}, bf16[512,128]{1,0:T(8,128)(2,1)S(1)}, u32[]{:S(2)}, u32[]{:S(2)}) collective-permute-start(bf16[512,128]{1,0:T(8,128)(2,1)S(1)} %slice_bitcast_fusion.4), channel_id=1, source_target_pairs={{0,2},{1,3},{2,0},{3,1},{4,6},{5,7},{6,4},{7,5},{8,10},{9,11},{10,... | collective-permute-start | bytes 393224 | tf_op jit(solution)/shard_map/ppermute | solution.py:118
  38.4 10.7 %collective-permute-start.17 = (bf16[512,128]{1,0:T(8,128)(2,1)S(1)}, bf16[512,128]{1,0:T(8,128)(2,1)S(1)}, u32[]{:S(2)}, u32[]{:S(2)}) collective-permute-start(bf16[512,128]{1,0:T(8,128)(2,1)S(1)} %slice_bitcast_fusion.2), channel_id=1, source_target_pairs={{0,2},{1,3},{2,0},{3,1},{4,6},{5,7},{6,4},{7,5},{8,10},{9,11},{10,... | collective-permute-start | bytes 393224 | tf_op jit(solution)/shard_map/ppermute | solution.py:118
  40.2 9.9 %collective-permute-start.20 = (bf16[512,128]{1,0:T(8,128)(2,1)S(1)}, bf16[512,128]{1,0:T(8,128)(2,1)S(1)}, u32[]{:S(2)}, u32[]{:S(2)}) collective-permute-start(bf16[512,128]{1,0:T(8,128)(2,1)S(1)} %slice_bitcast_fusion), channel_id=1, source_target_pairs={{0,2},{1,3},{2,0},{3,1},{4,6},{5,7},{6,4},{7,5},{8,10},{9,11},{10,... | collective-permute-start | bytes 393224 | tf_op jit(solution)/shard_map/ppermute | solution.py:118
  45.3 12.3 %collective-permute-start.15 = (bf16[512,128]{1,0:T(8,128)(2,1)S(1)}, bf16[512,128]{1,0:T(8,128)(2,1)S(1)}, u32[]{:S(2)}, u32[]{:S(2)}) collective-permute-start(bf16[512,128]{1,0:T(8,128)(2,1)S(1)} %fusion.2), channel_id=1, source_target_pairs={{0,8},{1,9},{2,10},{3,11},{4,12},{5,13},{6,14},{7,15},{8,0},{9,1},... | collective-permute-start | bytes 393224 | tf_op jit(solution)/shard_map/ppermute | solution.py:122
  49.1 8.6 %collective-permute-start.18 = (bf16[512,128]{1,0:T(8,128)(2,1)S(1)}, bf16[512,128]{1,0:T(8,128)(2,1)S(1)}, u32[]{:S(2)}, u32[]{:S(2)}) collective-permute-start(bf16[512,128]{1,0:T(8,128)(2,1)S(1)} %fusion.1), channel_id=1, source_target_pairs={{0,4},{1,5},{2,6},{3,7},{4,8},{5,9},{6,10},{7,11},{8,12},{9,13},{1... | collective-permute-start | bytes 393224 | tf_op jit(solution)/shard_map/ppermute | solution.py:122
  50.2 9.3 %collective-permute-start.21 = (bf16[512,128]{1,0:T(8,128)(2,1)S(1)}, bf16[512,128]{1,0:T(8,128)(2,1)S(1)}, u32[]{:S(2)}, u32[]{:S(2)}) collective-permute-start(bf16[512,128]{1,0:T(8,128)(2,1)S(1)} %fusion), channel_id=1, source_target_pairs={{0,12},{1,13},{2,14},{3,15},{4,0},{5,1},{6,2},{7,3},{8,4},{9,5},{1... | collective-permute-start | bytes 393224 | tf_op jit(solution)/shard_map/ppermute | solution.py:122
  59.7 1.2 %collective-permute-start.22 = (f32[512]{0:T(512)S(1)}, f32[512]{0:T(512)S(1)}, u32[]{:S(2)}, u32[]{:S(2)}) collective-permute-start(f32[512]{0:T(512)S(1)} %multiply_reduce_fusion), channel_id=1, source_target_pairs={{0,1},{1,0},{2,3},{3,2},{4,5},{5,4},{6,7},{7,6},{8,9},{9,8},{10,11... | collective-permute-start | bytes 6152 | tf_op jit(solution)/shard_map/ppermute | solution.py:118
  60.9 3.6 %collective-permute-start.23 = (f32[512]{0:T(512)S(1)}, f32[512]{0:T(512)S(1)}, u32[]{:S(2)}, u32[]{:S(2)}) collective-permute-start(f32[512]{0:T(512)S(1)} %add.65), channel_id=1, source_target_pairs={{0,2},{1,3},{2,0},{3,1},{4,6},{5,7},{6,4},{7,5},{8,10},{9,11},{10,... | collective-permute-start | bytes 6152 | tf_op jit(solution)/shard_map/ppermute | solution.py:118
  64.5 3.6 %collective-permute-start.26 = (f32[512]{0:T(512)S(1)}, f32[512]{0:T(512)S(1)}, u32[]{:S(2)}, u32[]{:S(2)}) collective-permute-start(f32[512]{0:T(512)S(1)} %add.66), channel_id=1, source_target_pairs={{0,12},{1,13},{2,14},{3,15},{4,0},{5,1},{6,2},{7,3},{8,4},{9,5},{1... | collective-permute-start | bytes 6152 | tf_op jit(solution)/shard_map/ppermute | solution.py:122
  65.6 4.5 %collective-permute-start.25 = (f32[512]{0:T(512)S(1)}, f32[512]{0:T(512)S(1)}, u32[]{:S(2)}, u32[]{:S(2)}) collective-permute-start(f32[512]{0:T(512)S(1)} %add.66), channel_id=1, source_target_pairs={{0,8},{1,9},{2,10},{3,11},{4,12},{5,13},{6,14},{7,15},{8,0},{9,1},... | collective-permute-start | bytes 6152 | tf_op jit(solution)/shard_map/ppermute | solution.py:122
  66.9 5.4 %collective-permute-start.24 = (f32[512]{0:T(512)S(1)}, f32[512]{0:T(512)S(1)}, u32[]{:S(2)}, u32[]{:S(2)}) collective-permute-start(f32[512]{0:T(512)S(1)} %add.66), channel_id=1, source_target_pairs={{0,4},{1,5},{2,6},{3,7},{4,8},{5,9},{6,10},{7,11},{8,12},{9,13},{1... | collective-permute-start | bytes 6152 | tf_op jit(solution)/shard_map/ppermute | solution.py:122
